TPU v7x, 128 devices: a whole 4x4x4 slice. The times are simulated.
128 devices in a mesh: ep: 32 (over z, y, core), tp: 4 (over x).
Axes of the slice: x: 4, y: 4, z: 4, core: 2. Of those that a mesh axis runs over, the one named last changes fastest.
Arguments:
- mix_input: bfloat16 [16384, 4096], P(('ep', 'tp')), may hold values from -30 to 30
- moe_input: bfloat16 [16384, 4096], P(('ep', 'tp')), may hold values from -6 to 6
- norm_mix: float32 [4096], replicated, may hold values from 0.1 to 1.9
- query_weight: bfloat16 [4096, 2048], P(None, 'tp'), may hold values from -0.09375 to 0.09375
- forget_weight: bfloat16 [4096, 2048], P(None, 'tp'), may hold values from -0.09375 to 0.09375
- value_weight: bfloat16 [4096, 2048], P(None, 'tp'), may hold values from -0.09375 to 0.09375
- forget_gap: float32 [2048], P('tp'), may hold values from 1e-05 to 0.06
- norm_out: float32 [2048], P('tp'), may hold values from 0.1 to 1.9
- norm_moe: float32 [4096], replicated, may hold values from 0.1 to 1.9
- router_weight: bfloat16 [4096, 32], replicated, may hold values from -0.09375 to 0.09375
- expert_gate: bfloat16 [32, 4096, 1024], P('ep', None, 'tp'), may hold values from -2 to 2, as said below
- expert_up: bfloat16 [32, 4096, 1024], P('ep', None, 'tp'), may hold values from -2 to 2, as said below
- expert_down: bfloat16 [32, 1024, 4096], P('ep', None, 'tp'), may hold values from -0.1875 to 0.1875
- routes: int32 [16384, 2], P('ep'), may hold values from 0 to 31, all different within a row; in each aligned block of 128 rows (0 to 127, 128 to 255, ...) at most 16 rows name the same one
Outputs:
- mixer_out: bfloat16 [16384, 2048], P('ep', 'tp')
- expert_out: bfloat16 [16384, 4096], P('ep', 'tp')
Inputs may be any that keep to these rules, and one draw needn't show every extreme that they name: `routes`: each row names 2 different experts; in each aligned block of 128 rows no expert is named by more than 16 rows. `expert_gate`: independent entries, scaled by the fan-in 4096. `expert_up`: independent entries, scaled by the fan-in 4096.
All inputs are finite; a program needn't handle non-finite values.
Results may differ from a plain program's by a relative error of at most 0.012.
The roundings to bfloat16 on the way count: a program that leaves them out, or rounds other values in their place, can miss the bound.
Values may be sent and summed in bfloat16 or wider, within the bound.
No kernel may reach another device: no remote copies, remote signals or barrier semaphores. Data moves between devices by JAX's collectives and lax.ppermute only.
A program may use at most 192 MiB of HBM per device.

v0:
```python
import jax
import jax.numpy as jnp
from jax import lax
from jax.sharding import Mesh
from jax.sharding import PartitionSpec as P

HEAD_DIM = 128
TOPK = 2
BLOCK = 64
EP = ("ep_0", "ep_1", "ep_2")
EP_TP = ("ep_0", "ep_1", "ep_2", "tp")


EPSILON = 1e-06
CLAMP_LIMIT = 7.0
SWISH_SLOPE = 1.702
MAXIMAL_ACCURACY = lax.Precision.HIGHEST


def side_by_side(arrays, axis, dim, along):
    ends, at = ([], 0)
    for a in arrays[:-1]:
        at += a.shape[along]
        ends.append(at)
    both = jnp.concatenate(arrays, axis=along)
    return tuple(jnp.split(lax.all_gather(both, axis, axis=dim, tiled=True), ends, axis=along))


def neutral_like(value, identity):
    return jax.tree.map(
        lambda part, zero: jnp.zeros_like(part) + jnp.asarray(zero, part.dtype), value, identity
    )


def entering(value, axes, combine, identity):
    before = start = neutral_like(value, identity)
    running = value
    for axis in reversed(axes):
        count, here = (lax.axis_size(axis), lax.axis_index(axis))
        pieces = jax.tree.map(lambda part: lax.all_gather(part, axis), running)
        inside, running = (start, start)
        for k in range(count):
            passed = k < here
            running = combine(running, jax.tree.map(lambda part: part[k], pieces))
            inside = jax.tree.map(lambda new, old: jnp.where(passed, new, old), running, inside)
        before = combine(inside, before)
    return before


def normed(row_data, gain_vec):
    as_float = row_data.astype(jnp.float32)
    scale = lax.rsqrt(jnp.mean(as_float * as_float, axis=-1, keepdims=True) + EPSILON)
    return as_float * scale * gain_vec


def head_blocks(matrix, head_count):
    row_count = matrix.shape[0]
    return matrix.reshape(row_count // BLOCK, BLOCK, head_count, HEAD_DIM).transpose(0, 2, 1, 3)


def block_pass(running_state, inputs):
    query_rows, key_matrix_rows, value_rows, log_forget = inputs
    prefix_log_decay = jnp.cumsum(log_forget, axis=1)
    places = jnp.arange(BLOCK, dtype=jnp.int32)
    causal = (places[:, None] >= places[None, :])[None, :, :, None]
    spread = prefix_log_decay[:, :, None, :] - prefix_log_decay[:, None, :, :]
    decays = jnp.exp(jnp.where(causal, spread, -jnp.inf))
    scores = jnp.einsum(
        "htk,hsk,htsk->hts", query_rows, key_matrix_rows, decays, precision=MAXIMAL_ACCURACY
    )
    inside = jnp.einsum("hts,hsv->htv", scores, value_rows, precision=MAXIMAL_ACCURACY)
    carried_state_block = jnp.einsum(
        "faq,fqp->fap",
        query_rows * jnp.exp(prefix_log_decay),
        running_state,
        precision=MAXIMAL_ACCURACY,
    )
    final_log_sum = prefix_log_decay[:, -1:, :]
    state_update = jnp.einsum(
        "fge,fga->fea",
        key_matrix_rows * jnp.exp(final_log_sum - prefix_log_decay),
        value_rows,
        precision=MAXIMAL_ACCURACY,
    )
    running_state = jnp.exp(final_log_sum[:, 0, :, None]) * running_state + state_update
    return (running_state, (inside + carried_state_block, prefix_log_decay))


def head_readout(block_out, gain_vec, head_count):
    block_total = block_out.shape[0]
    row_values = block_out.transpose(0, 2, 1, 3).reshape(block_total * BLOCK, head_count, HEAD_DIM)
    scale = lax.rsqrt(jnp.mean(row_values * row_values, axis=-1, keepdims=True) + EPSILON)
    shaped = row_values * scale * gain_vec.reshape(head_count, HEAD_DIM)
    return shaped.reshape(block_total * BLOCK, head_count * HEAD_DIM).astype(jnp.bfloat16)


def slot_places(routes, block_rows, expert_count, capacity):
    row_count = routes.shape[0]
    picks = routes.shape[1]
    flat_ids = routes.reshape(-1)
    onehot = (flat_ids[:, None] == jnp.arange(expert_count, dtype=jnp.int32)[None, :]).astype(
        jnp.int32
    )
    per_block = onehot.reshape(row_count // block_rows, block_rows * picks, expert_count)
    before = jnp.cumsum(per_block, axis=1) - per_block
    slot_rank = jnp.sum(before * per_block, axis=2).reshape(-1)
    anchor = jnp.arange(row_count * picks, dtype=jnp.int32) // (block_rows * picks)
    return (flat_ids * (row_count // block_rows) + anchor) * capacity + slot_rank


def route_weights(logits, routes):
    expert_count = logits.shape[1]
    chosen = routes[:, :, None] == jnp.arange(expert_count, dtype=jnp.int32)[None, None, :]
    picked = jnp.sum(jnp.where(chosen, logits.astype(jnp.float32)[:, None, :], 0.0), axis=2)
    differences = picked[:, None, :] - picked[:, :, None]
    return 1.0 / jnp.sum(jnp.exp(differences), axis=2)


def fill_slots(row_data, dest, slot_total):
    row_count = row_data.shape[0]
    per_row = dest.shape[0] // row_count
    source = (
        jnp.full((slot_total,), row_count, jnp.int32)
        .at[dest]
        .set(jnp.arange(dest.shape[0], dtype=jnp.int32) // per_row)
    )
    padded = jnp.concatenate([row_data, jnp.zeros((1, row_data.shape[1]), row_data.dtype)], axis=0)
    return padded[source]


def link_states(earlier, later_part):
    return (earlier[0] * later_part[0], later_part[0][:, :, None] * earlier[1] + later_part[1])


def per_device(
    mix_input,
    moe_input,
    norm_mix,
    query_weight,
    forget_weight,
    value_weight,
    forget_gap,
    norm_out,
    norm_moe,
    router_weight,
    expert_gate,
    expert_up,
    expert_down,
    routes,
):
    ep_count = lax.axis_size(EP)
    tp_count = lax.axis_size("tp")
    tok_dev = moe_input.shape[0]
    model_width = moe_input.shape[1]
    expert_count = router_weight.shape[1]
    local_experts = expert_gate.shape[0]
    capacity = 2 * tok_dev * TOPK // expert_count
    rows_a = normed(mix_input, norm_mix).astype(jnp.bfloat16)
    rows_b = normed(moe_input, norm_moe).astype(jnp.bfloat16)
    logits = jnp.dot(rows_b, router_weight, preferred_element_type=jnp.float32).astype(jnp.bfloat16)
    group_a, group_logits = side_by_side((rows_a, logits), "tp", 0, 1)
    head_count = query_weight.shape[1] // HEAD_DIM
    query_rows = jnp.dot(group_a, query_weight, preferred_element_type=jnp.float32)
    forget_pre = jnp.dot(group_a, forget_weight, preferred_element_type=jnp.float32)
    value_rows = jnp.dot(group_a, value_weight, preferred_element_type=jnp.float32)
    shut = forget_gap * jax.nn.sigmoid(-forget_pre)
    log_forget = jnp.log1p(-shut)
    query_block_tiles = head_blocks(query_rows, head_count)
    zero_state = jnp.zeros((head_count, HEAD_DIM, HEAD_DIM), jnp.float32)
    end_state, (inside, prefix_log_decay) = lax.scan(
        block_pass,
        zero_state,
        (
            query_block_tiles,
            head_blocks(shut, head_count),
            head_blocks(value_rows, head_count),
            head_blocks(log_forget, head_count),
        ),
    )
    totals = prefix_log_decay[:, :, -1, :]
    offsets = jnp.cumsum(totals, axis=0) - totals
    prefix_totals = prefix_log_decay + offsets[:, :, None, :]
    decay_total = jnp.exp(jnp.sum(totals, axis=0))
    identity = (jnp.ones_like(decay_total), jnp.zeros_like(end_state))
    incoming_decay, incoming_state = entering((decay_total, end_state), EP, link_states, identity)
    arriving = jnp.einsum(
        "xeqb,ebc->xeqc",
        query_block_tiles * jnp.exp(prefix_totals),
        incoming_state,
        precision=MAXIMAL_ACCURACY,
    )
    mixer_out = head_readout(inside + arriving, norm_out, head_count)
    group_rows = routes.shape[0]
    group_dest = slot_places(routes, tok_dev, expert_count, capacity)
    weights = route_weights(group_logits, routes)
    own_index = lax.axis_index("tp")
    own_routes = lax.dynamic_slice_in_dim(routes, own_index * tok_dev, tok_dev, 0)
    own_dest = slot_places(own_routes, tok_dev, expert_count, capacity)
    buffer = fill_slots(rows_b, own_dest, expert_count * capacity)
    outgoing = buffer.reshape(ep_count, local_experts, capacity, model_width)
    arrived = lax.all_to_all(outgoing, EP, split_axis=0, concat_axis=0, tiled=True)
    stacked = lax.all_gather(arrived, "tp", axis=2, tiled=True)
    gate_pre = jnp.einsum(
        "send,edf->senf", stacked, expert_gate, preferred_element_type=jnp.float32
    )
    up_pre = jnp.einsum("send,edf->senf", stacked, expert_up, preferred_element_type=jnp.float32)
    gated = jnp.minimum(gate_pre, CLAMP_LIMIT)
    opened = jnp.clip(up_pre, -CLAMP_LIMIT, CLAMP_LIMIT)
    hidden = ((opened + 1.0) * gated * jax.nn.sigmoid(SWISH_SLOPE * gated)).astype(jnp.bfloat16)
    summed = jnp.einsum(
        "senf,efc->senc",
        lax.all_gather(hidden, "tp", axis=3, tiled=True),
        expert_down,
        preferred_element_type=jnp.float32,
    )
    returned = lax.all_to_all(
        summed.astype(jnp.bfloat16), EP, split_axis=0, concat_axis=0, tiled=True
    )
    flat_results = returned.reshape(expert_count * tp_count * capacity, returned.shape[3])
    picked = (
        flat_results[group_dest].reshape(group_rows, TOPK, returned.shape[3]).astype(jnp.float32)
    )
    expert_out = jnp.sum(weights[:, :, None] * picked, axis=1).astype(jnp.bfloat16)
    return (mixer_out, expert_out)


def solution(mesh):
    finer = Mesh(mesh.devices.reshape(4, 4, 2, mesh.shape["tp"]), ("ep_0", "ep_1", "ep_2", "tp"))
    placed = (
        P(EP_TP, None),
        P(EP_TP, None),
        P(),
        P(None, "tp"),
        P(None, "tp"),
        P(None, "tp"),
        P("tp"),
        P("tp"),
        P(),
        P(),
        P(EP, None, "tp"),
        P(EP, None, "tp"),
        P(EP, None, "tp"),
        P(EP, None),
    )
    return jax.shard_map(
        per_device,
        mesh=finer,
        in_specs=placed,
        out_specs=(P(EP, "tp"), P(EP, "tp")),
        check_vma=False,
    )
```

profile of v0, /device:TPU:8, one launch (start us, length us, event | category | flops | bytes accessed | tf_op | source)
XLA Modules:
  0.0 518.1 jit_solution(6898131361314549228)
XLA Ops:
  7.3 1.7 fusion.38
  20.4 4.4 gather_fusion
  24.8 58.4 %all_to_all.10 = bf16[32,1,16,4096]{3,2,1,0:T(8,128)(2,1)} all-to-all(bf16[32,1,16,4096]{3,2,1,0:T(8,128)(2,1)} %bitcast.341), channel_id=1, replica_groups=mesh['ep_0'=4,'ep_1'=4,'ep_2'=2,'tp'=4] {'ep_0','ep_1','ep_2'}, dimensions={0} | all-to-all | bytes 8388608 | tf_op jit(solution)/shard_map/all_to_all | solution.py:201
  83.5 5.8 %fusion.29 = f32[512,512]{1,0:T(8,128)S(1)} fusion(bf16[4096,512]{1,0:T(8,128)(2,1)} %param.21, bf16[512,4128]{0,1:T(8,128)(2,1)} %all-gather.11.cloned.1.call-done), kind=kOutput, calls=%fused_computation.45 | convolution fusion | flops 2147483648 | bytes 9437184 | tf_op jit(solution)/shard_map/dot_general | solution.py:165
  90.7 8.2 %fusion.27 = f32[512,512]{1,0:T(8,128)} fusion(bf16[4096,512]{1,0:T(8,128)(2,1)} %param.19, bf16[512,4128]{0,1:T(8,128)(2,1)} %all-gather.11.cloned.1.call-done), kind=kOutput, calls=%fused_computation.43 | convolution fusion | flops 2147483648 | bytes 9437184 | tf_op jit(solution)/shard_map/dot_general | solution.py:163
  98.8 1.7 reshape.468
  100.5 8.6 %negate_log-plus-one_fusion = (f32[512,512]{1,0:T(8,128)}, f32[512,512]{1,0:T(8,128)}) fusion(bf16[4096,512]{1,0:T(8,128)(2,1)} %param.20, bf16[512,4128]{0,1:T(8,128)(2,1)} %all-gather.11.cloned.1.call-done, f32[512]{0:T(512)S(1)} %copy-done.13), kind=kOutput, calls=%fused_computation.84 | convolution fusion | flops 2148532224 | bytes 10487808 | tf_op jit(solution)/shard_map/dot_general | solution.py:164
  109.1 2.5 reshape.465
  111.6 2.6 reshape.466
  114.2 3.3 copy_bitcast_fusion.2
  117.5 1.6 copy_bitcast_fusion
  119.1 116.8 %all-gather.17.cloned.1.call-done = bf16[32,1,64,4096]{3,2,0,1:T(8,128)(2,1)} async-done(((bf16[32,1,16,4096]{3,2,0,1:T(8,128)(2,1)}), bf16[32,1,64,4096]{3,2,0,1:T(8,128)(2,1)}) %all-gather.17.cloned.1.call-update) | async-done | bytes 16777232 | tf_op jit(solution)/shard_map/all_gather | solution.py:202
  236.0 9.2 %fusion.21 = f32[32,64,256]{2,1,0:T(8,128)S(1)} fusion(bf16[32,1,64,4096]{3,2,0,1:T(8,128)(2,1)} %all-gather.17.cloned.1.call-done, bf16[1,4096,256]{2,1,0:T(8,128)(2,1)} %param.26), kind=kOutput, calls=%fused_computation.35 | convolution fusion | flops 4294967296 | bytes 20971520 | tf_op jit(solution)/shard_map/send,edf->senf/dot_general | solution.py:203
  245.1 2.0 copy-done.11
  247.7 6.2 %fusion.53 = bf16[32,1,64,256]{3,2,0,1:T(8,128)(2,1)} fusion(f32[32,64,256]{2,1,0:T(8,128)S(1)} %fusion.21, bf16[1,4096,256]{2,1,0:T(8,128)(2,1)S(1)} %copy-done.12, bf16[32,1,64,4096]{3,2,0,1:T(8,128)(2,1)S(1)} %copy-done.11), kind=kOutput, calls=%fused_computation.67 | convolution fusion | flops 4300210176 | bytes 22020096 | tf_op jit(solution)/shard_map/send,edf->senf/dot_general | solution.py:206
  254.0 132.5 %while.15 = (s32[]{:T(128)}, f32[4,128,128]{2,1,0:T(8,128)S(1)}, f32[8,4,64,128]{3,2,0,1:T(8,128)}, f32[8,4,64,128]{3,2,1,0:T(8,128)}, f32[8,4,64,128]{3,2,1,0:T...) while((s32[]{:T(128)}, f32[4,128,128]{2,1,0:T(8,128)S(1)}, ...), condition=%wide.region_4.5_spmd.clone, body=%wide.region_2.4_spmd.clone.sunk | while | flops 138760192 | bytes 20602000 | solution.py:170
  258.5 7.4 %fusion.173 = f32[4,64,64]{1,2,0:T(8,128)S(1)} fusion(f32[4,64,64,128]{3,2,1,0:T(8,128)S(1)} %select_exponential_fusion.2, f32[4,128,64]{1,2,0:T(8,128)S(1)} %get-tuple-element.166, f32[4,128,64]{1,2,0:T(8,128)S(1)} %dynamic-slice_bitcast_fusion.6), kind=kLoop, calls=%fused_computation.4.clone.1 | loop fusion | flops 6275072 | bytes 8716288 | tf_op jit(solution)/shard_map/while/body/eval_jaxpr/htk,hsk,htsk->hts/dot_general | solution.py:68
  267.2 1.9 fusion.175
  269.2 1.6 convolution_add_fusion.3
  275.1 7.4 %fusion.173 = f32[4,64,64]{1,2,0:T(8,128)S(1)} fusion(f32[4,64,64,128]{3,2,1,0:T(8,128)S(1)} %select_exponential_fusion.2, f32[4,128,64]{1,2,0:T(8,128)S(1)} %get-tuple-element.166, f32[4,128,64]{1,2,0:T(8,128)S(1)} %dynamic-slice_bitcast_fusion.6), kind=kLoop, calls=%fused_computation.4.clone.1 | loop fusion | flops 6275072 | bytes 8716288 | tf_op jit(solution)/shard_map/while/body/eval_jaxpr/htk,hsk,htsk->hts/dot_general | solution.py:68
  283.8 1.9 fusion.175
  291.6 7.4 %fusion.173 = f32[4,64,64]{1,2,0:T(8,128)S(1)} fusion(f32[4,64,64,128]{3,2,1,0:T(8,128)S(1)} %select_exponential_fusion.2, f32[4,128,64]{1,2,0:T(8,128)S(1)} %get-tuple-element.166, f32[4,128,64]{1,2,0:T(8,128)S(1)} %dynamic-slice_bitcast_fusion.6), kind=kLoop, calls=%fused_computation.4.clone.1 | loop fusion | flops 6275072 | bytes 8716288 | tf_op jit(solution)/shard_map/while/body/eval_jaxpr/htk,hsk,htsk->hts/dot_general | solution.py:68
  300.3 1.9 fusion.175
  308.2 7.4 %fusion.173 = f32[4,64,64]{1,2,0:T(8,128)S(1)} fusion(f32[4,64,64,128]{3,2,1,0:T(8,128)S(1)} %select_exponential_fusion.2, f32[4,128,64]{1,2,0:T(8,128)S(1)} %get-tuple-element.166, f32[4,128,64]{1,2,0:T(8,128)S(1)} %dynamic-slice_bitcast_fusion.6), kind=kLoop, calls=%fused_computation.4.clone.1 | loop fusion | flops 6275072 | bytes 8716288 | tf_op jit(solution)/shard_map/while/body/eval_jaxpr/htk,hsk,htsk->hts/dot_general | solution.py:68
  316.9 1.9 fusion.175
  324.7 7.4 %fusion.173 = f32[4,64,64]{1,2,0:T(8,128)S(1)} fusion(f32[4,64,64,128]{3,2,1,0:T(8,128)S(1)} %select_exponential_fusion.2, f32[4,128,64]{1,2,0:T(8,128)S(1)} %get-tuple-element.166, f32[4,128,64]{1,2,0:T(8,128)S(1)} %dynamic-slice_bitcast_fusion.6), kind=kLoop, calls=%fused_computation.4.clone.1 | loop fusion | flops 6275072 | bytes 8716288 | tf_op jit(solution)/shard_map/while/body/eval_jaxpr/htk,hsk,htsk->hts/dot_general | solution.py:68
  333.4 1.9 fusion.175
  341.2 7.4 %fusion.173 = f32[4,64,64]{1,2,0:T(8,128)S(1)} fusion(f32[4,64,64,128]{3,2,1,0:T(8,128)S(1)} %select_exponential_fusion.2, f32[4,128,64]{1,2,0:T(8,128)S(1)} %get-tuple-element.166, f32[4,128,64]{1,2,0:T(8,128)S(1)} %dynamic-slice_bitcast_fusion.6), kind=kLoop, calls=%fused_computation.4.clone.1 | loop fusion | flops 6275072 | bytes 8716288 | tf_op jit(solution)/shard_map/while/body/eval_jaxpr/htk,hsk,htsk->hts/dot_general | solution.py:68
  349.9 1.9 fusion.175
  357.8 7.4 %fusion.173 = f32[4,64,64]{1,2,0:T(8,128)S(1)} fusion(f32[4,64,64,128]{3,2,1,0:T(8,128)S(1)} %select_exponential_fusion.2, f32[4,128,64]{1,2,0:T(8,128)S(1)} %get-tuple-element.166, f32[4,128,64]{1,2,0:T(8,128)S(1)} %dynamic-slice_bitcast_fusion.6), kind=kLoop, calls=%fused_computation.4.clone.1 | loop fusion | flops 6275072 | bytes 8716288 | tf_op jit(solution)/shard_map/while/body/eval_jaxpr/htk,hsk,htsk->hts/dot_general | solution.py:68
  366.5 1.9 fusion.175
  374.3 7.4 %fusion.173 = f32[4,64,64]{1,2,0:T(8,128)S(1)} fusion(f32[4,64,64,128]{3,2,1,0:T(8,128)S(1)} %select_exponential_fusion.2, f32[4,128,64]{1,2,0:T(8,128)S(1)} %get-tuple-element.166, f32[4,128,64]{1,2,0:T(8,128)S(1)} %dynamic-slice_bitcast_fusion.6), kind=kLoop, calls=%fused_computation.4.clone.1 | loop fusion | flops 6275072 | bytes 8716288 | tf_op jit(solution)/shard_map/while/body/eval_jaxpr/htk,hsk,htsk->hts/dot_general | solution.py:68
  383.0 1.9 fusion.175
  387.5 1.8 all-gather.3
  389.3 10.8 %all-gather.4 = f32[4,4,128]{2,1,0:T(4,128)S(1)} all-gather(f32[1,4,128]{2,1,0:T(4,128)S(1)} %fusion.154), channel_id=4, replica_groups=mesh['ep_0'=4,'ep_1'=4,'ep_2'=2,'tp'=4] {'ep_1'}, dimensions={0}, use_global_device_ids=true | all-gather | bytes 10240 | tf_op jit(solution)/shard_map/all_gather | solution.py:40
  400.2 2.2 all-gather.1
  404.1 8.8 %convert_bitcast_fusion = bf16[32,1,64,1024]{3,2,1,0:T(8,128)(2,1)} fusion(bf16[32,1,64,1024]{3,2,0,1:T(8,128)(2,1)} %all-gather.19.cloned.1.call-done, bf16[1,1024,1024]{2,1,0:T(8,128)(2,1)S(1)} %copy-done), kind=kOutput, calls=%fused_computation.42 | convolution fusion | flops 4297064448 | bytes 10485760 | tf_op jit(solution)/shard_map/senf,efc->senc/dot_general | solution.py:210
  412.9 7.0 %all-to-all-start.1 = ((bf16[32,1,64,1024]{3,2,1,0:T(8,128)(2,1)}), bf16[32,1,64,1024]{3,2,1,0:T(8,128)(2,1)}, u32[]{:S(2)}, u32[]{:S(2)}) async-start(bf16[32,1,64,1024]{3,2,1,0:T(8,128)(2,1)} %convert_bitcast_fusion), calls=%async_computation.1 | async-start | bytes 8388608 | tf_op jit(solution)/shard_map/all_to_all | solution.py:216
  420.8 2.3 reduce-window.16
  423.5 9.5 %all-gather.13.cloned.1.call-done = f32[4,4,128,128]{3,2,1,0:T(8,128)} async-done(((f32[1,4,128,128]{3,2,1,0:T(8,128)}), f32[4,4,128,128]{3,2,1,0:T(8,128)}) %all-gather.13.cloned.1.call-update) | async-done | bytes 1048592 | tf_op jit(solution)/shard_map/all_gather | solution.py:40
  433.0 2.2 multiply_add_fusion
  436.3 33.6 %all_gather.38 = f32[4,4,128]{2,1,0:T(4,128)S(1)} all-gather(f32[1,4,128]{2,1,0:T(4,128)S(1)} %get-tuple-element.100), channel_id=1, replica_groups=mesh['ep_0'=4,'ep_1'=4,'ep_2'=2,'tp'=4] {'ep_0'}, dimensions={0}, use_global_device_ids=true | all-gather | bytes 10240 | tf_op jit(solution)/shard_map/all_gather | solution.py:40
  471.0 8.4 %all-gather.15.cloned.1.call-done = f32[4,4,128,128]{3,2,1,0:T(8,128)} async-done(((f32[1,4,128,128]{3,2,1,0:T(8,128)}), f32[4,4,128,128]{3,2,1,0:T(8,128)}) %all-gather.15.cloned.1.call-update) | async-done | bytes 1048592 | tf_op jit(solution)/shard_map/all_gather | solution.py:40
  479.5 5.2 multiply_reduce_fusion.1
  484.8 1.9 copy.106
  488.4 8.9 %gather_fusion.1 = bf16[1024,1024]{1,0:T(8,128)(2,1)} fusion(bf16[2048,1024]{1,0:T(8,128)(2,1)} %bitcast.60, s32[1024]{0:T(1024)S(1)} %broadcast_clamp_fusion), kind=kCustom, calls=%fused_computation.1 | custom fusion | bytes 4198400 | tf_op jit(solution)/shard_map/gather | solution.py:221
  497.3 5.5 %reshape.486 = f32[512,2,1024]{2,1,0:T(2,128)} reshape(bf16[1024,1024]{1,0:T(8,128)(2,1)} %gather_fusion.1) | data formatting | bytes 6291456 | tf_op jit(solution)/shard_map/convert_element_type | solution.py:221
  502.8 8.6 %multiply_reduce_fusion = bf16[512,1024]{1,0:T(8,128)(2,1)} fusion(f32[512,2,1024]{2,1,0:T(2,128)} %reshape.486, f32[512,2]{1,0:T(8,128)S(1)} %copy.108), kind=kLoop, calls=%fused_computation.41 | loop fusion | flops 1572864 | bytes 5246976 | tf_op jit(solution)/shard_map/reduce_sum | solution.py:223
  (185 shorter events, 77.1 us)
Async XLA Ops:
  7.2 397.0 %copy-start = (bf16[1,1024,1024]{2,1,0:T(8,128)(2,1)S(1)}, bf16[1,1024,1024]{2,1,0:T(8,128)(2,1)}, u32[]{:S(2)}) copy-start(bf16[1,1024,1024]{2,1,0:T(8,128)(2,1)} %param.28) | copy-start | bytes 6291460
  7.2 3.9 copy-start.8
  7.2 6.5 %copy-start.6 = (bf16[4096,32]{0,1:T(8,128)(2,1)S(1)}, bf16[4096,32]{0,1:T(8,128)(2,1)}, u32[]{:S(2)}) copy-start(bf16[4096,32]{0,1:T(8,128)(2,1)} %param.25) | copy-start | bytes 786436
  7.2 6.9 %copy-start.9 = (f32[4096]{0:T(1024)S(1)}, f32[4096]{0:T(1024)}, u32[]{:S(2)}) copy-start(f32[4096]{0:T(1024)} %param.18) | copy-start | bytes 49156
  7.2 76.2 %all-gather.11.cloned.1.call-start = ((), (), s32[]{:S(2)}) async-start(), calls=%async_computation.2 | async-start | bytes 5283840 | tf_op jit(solution)/shard_map/all_gather | solution.py:26
  11.1 4.9 copy-start.7
  12.7 1.0 copy-start.1
  15.9 220.0 %all-gather.17.cloned.1.call-start = ((), (), s32[]{:S(2)}) async-start(), calls=%async_computation.5 | async-start | bytes 20971520 | tf_op jit(solution)/shard_map/all_gather | solution.py:202
  83.2 320.9 %all-gather.19.cloned.1.call-start = ((), (), s32[]{:S(2)}) async-start(), calls=%async_computation.6 | async-start | bytes 5242880 | tf_op jit(solution)/shard_map/all_gather | solution.py:212
  90.7 9.9 %copy-start.13 = (f32[512]{0:T(512)S(1)}, f32[512]{0:T(512)}, u32[]{:S(2)}) copy-start(f32[512]{0:T(512)} %param.22) | copy-start | bytes 6148
  100.5 17.0 %copy-start.2 = (f32[8,64,4,128]{3,2,1,0:T(4,128)}, f32[8,64,4,128]{3,2,1,0:T(4,128)S(1)}, u32[]{:S(2)}) copy-start(f32[8,64,4,128]{3,2,1,0:T(4,128)S(1)} %reshape.468) | copy-start | bytes 3145732
  114.2 3.3 copy-start.4
  236.0 11.1 %copy-start.11 = (bf16[32,1,64,4096]{3,2,0,1:T(8,128)(2,1)S(1)}, bf16[32,1,64,4096]{3,2,0,1:T(8,128)(2,1)}, u32[]{:S(2)}) copy-start(bf16[32,1,64,4096]{3,2,0,1:T(8,128)(2,1)} %all-gather.17.cloned.1.call-done) | copy-start | bytes 50331652
  236.0 11.7 %copy-start.12 = (bf16[1,4096,256]{2,1,0:T(8,128)(2,1)S(1)}, bf16[1,4096,256]{2,1,0:T(8,128)(2,1)}, u32[]{:S(2)}) copy-start(bf16[1,4096,256]{2,1,0:T(8,128)(2,1)} %param.27) | copy-start | bytes 6291460
  254.0 179.0 %all-gather.13.cloned.1.call-start = ((), (), s32[]{:S(2)}) async-start(), calls=%async_computation.3 | async-start | bytes 1310720 | tf_op jit(solution)/shard_map/all_gather | solution.py:40
  402.4 0.8 copy-start.5
  412.9 75.5 %all-to-all-start.1 = ((bf16[32,1,64,1024]{3,2,1,0:T(8,128)(2,1)}), bf16[32,1,64,1024]{3,2,1,0:T(8,128)(2,1)}, u32[]{:S(2)}, u32[]{:S(2)}) async-start(bf16[32,1,64,1024]{3,2,1,0:T(8,128)(2,1)} %convert_bitcast_fusion), calls=%async_computation.1 | async-start | bytes 8388608 | tf_op jit(solution)/shard_map/all_to_all | solution.py:216
  419.9 59.6 %copy-start.3 = (f32[8,64,4,128]{3,2,1,0:T(4,128)S(1)}, f32[8,64,4,128]{3,2,1,0:T(4,128)}, u32[]{:S(2)}) copy-start(f32[8,64,4,128]{3,2,1,0:T(4,128)} %copy-done.2) | copy-start | bytes 3145732
  419.9 59.6 %all-gather.15.cloned.1.call-start = ((), (), s32[]{:S(2)}) async-start(), calls=%async_computation.4 | async-start | bytes 1310720 | tf_op jit(solution)/shard_map/all_gather | solution.py:40
  479.5 7.8 %copy-start.10 = (f32[512]{0:T(512)S(1)}, f32[512]{0:T(512)}, u32[]{:S(2)}) copy-start(f32[512]{0:T(512)} %param.23) | copy-start | bytes 6148
Sparse Core Ops, SparseCore 0:
  16.1 53.8 all-gather.10
  83.3 152.6 all-gather.16
  254.1 52.2 all-gather.18
  404.2 28.7 all-gather.12
  435.4 44.0 all-gather.14
where the time goes:
time: 524 us; the launch traced here: 518 us
  waiting for transfers between devices  135 us (26%)
  blocking collectives  107 us (20%)
  other arithmetic  96.7 us (18%)
  matrix products  91.2 us (17%)
  local copies, waits for them, and re-layouts  66 us (13%)
  between operations  14.4 us (3%)
  starting transfers between devices  7.35 us (1%)
    all_gather x1, waiting for transfers between devices, per_device(): stacked = lax.all_gather(arrived, 'tp', axis=2, tiled=True)  117 us
    dot_general x8, other arithmetic, block_pass(): jnp.einsum('htk,hsk,htsk->hts', query_rows, key_matrix_rows, decays, prec...  59.1 us
    all_to_all x1, blocking collectives, per_device(): lax.all_to_all(outgoing, EP, split_axis=0, concat_axis=0, tiled=True)  58.4 us
    all_gather x4, blocking collectives, entering(): pieces = jax.tree.map(lambda part: lax.all_gather(part, axis), running)  48.5 us
    all_gather x2, waiting for transfers between devices, entering(): pieces = jax.tree.map(lambda part: lax.all_gather(part, axis), running)  17.9 us
    dot_general x8, matrix products, block_pass(): jnp.einsum('faq,fqp->fap', query_rows * jnp.exp(prefix_log_decay), runnin...  15.5 us
    squeeze x16, local copies, waits for them, and re-layouts, per_device(): lax.scan(block_pass, zero_state, (query_block_tiles, head_blocks(shut, he...  15.3 us
    dot_general x8, matrix products, block_pass(): jnp.einsum('fge,fga->fea', key_matrix_rows * jnp.exp(final_log_sum - pref...  13 us
  transfers between devices with their start and end apart: 6, of which 3 were waited for; matrix products, arithmetic and copies ran while one was open for 39% of the time, Pallas kernels for 0%

commit v1 on v0

v1 whole, which is shorter than its diff:
```python
import jax
import jax.numpy as jnp
from jax import lax
from jax.experimental import pallas as pl
from jax.experimental.pallas import tpu as pltpu
from jax.sharding import Mesh
from jax.sharding import PartitionSpec as P

HEAD_DIM = 128
CAP = 16
EP = ("ep_0", "ep_1", "ep_2")
EP_TP = ("ep_0", "ep_1", "ep_2", "tp")

EPSILON = 1e-06
CLAMP_LIMIT = 7.0
SWISH_SLOPE = 1.702
EXACT = lax.Precision.HIGHEST
F32 = jnp.float32
BF16 = jnp.bfloat16


def mm(a, b, contract=((1,), (0,)), precision=None):
    return lax.dot_general(
        a, b, (contract, ((), ())), precision=precision, preferred_element_type=F32
    )


def params(mib=56, axes=("arbitrary",)):
    return pltpu.CompilerParams(vmem_limit_bytes=mib << 20, dimension_semantics=axes)


def normed(row_data, gain_vec):
    as_float = row_data.astype(F32)
    scale = lax.rsqrt(jnp.mean(as_float * as_float, axis=-1, keepdims=True) + EPSILON)
    return as_float * scale * gain_vec


def chosen(routes, experts):
    toks = routes.shape[1]
    ids = lax.broadcasted_iota(jnp.int32, (experts, toks), 0)
    first = routes[0:1, :] == ids
    second = routes[1:2, :] == ids
    count = jnp.where(first | second, 1.0, 0.0)
    earlier = (
        lax.broadcasted_iota(jnp.int32, (toks, toks), 0)
        < lax.broadcasted_iota(jnp.int32, (toks, toks), 1)
    )
    before = mm(count.astype(BF16), jnp.where(earlier, 1.0, 0.0).astype(BF16))
    return first, second, count, before


def slot_matrix(weight, before, count):
    experts, toks = weight.shape
    place = lax.broadcasted_iota(jnp.int32, (experts, CAP, toks), 1).astype(F32)
    here = (before[:, None, :] == place) & (count[:, None, :] > 0.5)
    return jnp.where(here, weight[:, None, :], 0.0).reshape(experts * CAP, toks)


def front_kernel(which, x_ref, gain_ref, router_ref, routes_ref, rows_ref, logits_ref, buf_ref, *, group):
    step = pl.program_id(0)

    @pl.when(step == 0)
    def _():
        rows_ref[...] = normed(x_ref[...], gain_ref[...]).astype(BF16)
        logits_ref[...] = mm(rows_ref[...], router_ref[...]).astype(BF16)

    fill(step, routes_ref, rows_ref, buf_ref, group)


def fill(step, routes_ref, rows_ref, buf_ref, group):
    experts = buf_ref.shape[0]
    routes = routes_ref[0] - step * group
    _, _, count, before = chosen(routes, experts)
    pick = slot_matrix(count, before, count).astype(BF16)
    buf_ref[...] = mm(pick, rows_ref[...]).astype(BF16).reshape(buf_ref.shape)


def fill_kernel(which, rows_ref, routes_ref, buf_ref, *, group):
    fill(pl.program_id(0), routes_ref, rows_ref, buf_ref, group)


def front(which, x, gain, router, routes, experts):
    toks, width = x.shape
    group = 8
    whole = lambda i, w: (0, 0)
    import functools

    return pl.pallas_call(
        functools.partial(front_kernel, group=group),
        grid_spec=pltpu.PrefetchScalarGridSpec(
            num_scalar_prefetch=1,
            grid=(experts // group,),
            in_specs=[
                pl.BlockSpec((toks, width), whole),
                pl.BlockSpec((1, width), whole),
                pl.BlockSpec(router.shape, whole),
                pl.BlockSpec((1, 2, toks), lambda i, w: (w[0], 0, 0)),
            ],
            out_specs=[
                pl.BlockSpec((toks, width), whole),
                pl.BlockSpec((toks, experts), whole),
                pl.BlockSpec((group, CAP, width), lambda i, w: (i, 0, 0)),
            ],
        ),
        out_shape=[
            jax.ShapeDtypeStruct((toks, width), BF16),
            jax.ShapeDtypeStruct((toks, experts), BF16),
            jax.ShapeDtypeStruct((experts, CAP, width), BF16),
        ],
        compiler_params=params(),
        name="front",
    )(which, x, gain, router, routes)


def refill(which, rows, routes, experts):
    toks, width = rows.shape
    group = 8
    import functools

    return pl.pallas_call(
        functools.partial(fill_kernel, group=group),
        grid_spec=pltpu.PrefetchScalarGridSpec(
            num_scalar_prefetch=1,
            grid=(experts // group,),
            in_specs=[
                pl.BlockSpec((toks, width), lambda i, w: (0, 0)),
                pl.BlockSpec((1, 2, toks), lambda i, w: (w[0], 0, 0)),
            ],
            out_specs=pl.BlockSpec((group, CAP, width), lambda i, w: (i, 0, 0)),
        ),
        out_shape=jax.ShapeDtypeStruct((experts, CAP, width), BF16),
        compiler_params=params(),
        name="refill",
    )(which, rows, routes)


def mixer_kernel(a_ref, q_ref, f_ref, v_ref, gap_ref, inside_ref, query_ref, packed_ref, qa, fa, va):
    step = pl.program_id(0)

    @pl.when(step == 0)
    def _():
        qa[...] = jnp.zeros_like(qa)
        fa[...] = jnp.zeros_like(fa)
        va[...] = jnp.zeros_like(va)

    a = a_ref[...]
    qa[...] += mm(a, q_ref[...])
    fa[...] += mm(a, f_ref[...])
    va[...] += mm(a, v_ref[...])

    @pl.when(step == pl.num_programs(0) - 1)
    def _():
        rows = a.shape[0]
        causal = (
            lax.broadcasted_iota(jnp.int32, (rows, rows), 0)
            >= lax.broadcasted_iota(jnp.int32, (rows, rows), 1)
        )
        ones = jnp.where(causal, 1.0, 0.0)
        heads = packed_ref.shape[0]
        for h in range(heads):
            at = slice(h * HEAD_DIM, (h + 1) * HEAD_DIM)
            shut = gap_ref[:, at] * jax.nn.sigmoid(-fa[:, at])
            sums = mm(ones, jnp.log1p(-shut), precision=EXACT)
            last = sums[rows - 1 :, :]
            value = va[:, at]
            query = qa[:, at] * jnp.exp(sums)
            scores = mm(query, shut * jnp.exp(-sums), ((1,), (1,)), EXACT)
            scores = jnp.where(causal, scores, 0.0)
            inside_ref[:, at] = mm(scores, value, precision=EXACT)
            query_ref[:, at] = query
            packed_ref[h, :HEAD_DIM, :] = mm(
                value, shut * jnp.exp(last - sums), ((0,), (0,)), EXACT
            )
            packed_ref[h, HEAD_DIM:, :] = jnp.broadcast_to(last, (8, HEAD_DIM))


def mixer(a, wq, wf, wv, gap):
    rows, width = a.shape
    cols = wq.shape[1]
    heads = cols // HEAD_DIM
    kb = 512
    fixed = lambda i: (0, 0)
    weight = pl.BlockSpec((kb, cols), lambda i: (i, 0))
    return pl.pallas_call(
        mixer_kernel,
        grid=(width // kb,),
        in_specs=[
            pl.BlockSpec((rows, kb), lambda i: (0, i)),
            weight,
            weight,
            weight,
            pl.BlockSpec((1, cols), fixed),
        ],
        out_specs=[
            pl.BlockSpec((rows, cols), fixed),
            pl.BlockSpec((rows, cols), fixed),
            pl.BlockSpec((heads, HEAD_DIM + 8, HEAD_DIM), lambda i: (0, 0, 0)),
        ],
        out_shape=[
            jax.ShapeDtypeStruct((rows, cols), F32),
            jax.ShapeDtypeStruct((rows, cols), F32),
            jax.ShapeDtypeStruct((heads, HEAD_DIM + 8, HEAD_DIM), F32),
        ],
        scratch_shapes=[pltpu.VMEM((rows, cols), F32)] * 3,
        compiler_params=params(),
        name="mixer",
    )(a, wq, wf, wv, gap)


def readout_kernel(inside_ref, query_ref, state_ref, gain_ref, out_ref):
    total = inside_ref[...] + mm(query_ref[...], state_ref[0], ((1,), (1,)), EXACT)
    out_ref[...] = normed(total, gain_ref[...]).astype(BF16)


def readout(inside, query, state, gain):
    rows, cols = inside.shape
    block = pl.BlockSpec((rows, HEAD_DIM), lambda h: (0, h))
    return pl.pallas_call(
        readout_kernel,
        grid=(cols // HEAD_DIM,),
        in_specs=[
            block,
            block,
            pl.BlockSpec((1, HEAD_DIM, HEAD_DIM), lambda h: (h, 0, 0)),
            pl.BlockSpec((1, HEAD_DIM), lambda h: (0, h)),
        ],
        out_specs=block,
        out_shape=jax.ShapeDtypeStruct((rows, cols), BF16),
        compiler_params=params(),
        name="readout",
    )(inside, query, state, gain)


def pieces(packed):
    return packed[:, HEAD_DIM : HEAD_DIM + 1, :], packed[:, :HEAD_DIM, :]


def link(earlier, later):
    return earlier[0] + later[0], jnp.exp(later[0]) * earlier[1] + later[1]


def pack(part):
    heads = part[1].shape[0]
    return jnp.concatenate(
        [part[1], jnp.broadcast_to(part[0], (heads, 8, HEAD_DIM))], axis=1
    )


def masked(flag, part):
    return jax.tree.map(lambda a: jnp.where(flag, a, 0.0), part)


def arriving_state(packed):
    core = lax.axis_index("ep_2")
    row = lax.axis_index("ep_1")
    other = lax.ppermute(packed, "ep_2", [(0, 1), (1, 0)])
    is_second = core == 1
    low = jnp.where(is_second, other, packed)
    high = jnp.where(is_second, packed, other)
    half = packed.shape[0] // 2
    mine = lambda a: lax.dynamic_slice_in_dim(a, core * half, half, 0)
    chip = link(pieces(mine(low)), pieces(mine(high)))
    count = lax.axis_size("ep_1")
    sent = pack(chip)
    before = after = None
    for d in range(count - 1, 0, -1):
        came = pieces(lax.ppermute(sent, "ep_1", [(i, (i + d) % count) for i in range(count)]))
        early = masked(row >= d, came)
        late = masked(row < d, came)
        before = early if before is None else link(before, early)
        after = late if after is None else link(after, late)
    plane = pack(link(link(before, chip), after))
    planes = None
    count = lax.axis_size("ep_0")
    for d in range(count - 1, 0, -1):
        came = pieces(lax.ppermute(plane, "ep_0", [(i, i + d) for i in range(count - d)]))
        planes = came if planes is None else link(planes, came)
    state = link(planes, before)[1]
    swapped = lax.ppermute(state, "ep_2", [(0, 1), (1, 0)])
    entering = jnp.concatenate(
        [jnp.where(is_second, swapped, state), jnp.where(is_second, state, swapped)], axis=0
    )
    first_core = pieces(low)
    return jnp.where(is_second, jnp.exp(first_core[0]) * entering + first_core[1], entering)


def hidden_kernel(rows_ref, go_ref, uo_ref, gr_ref, ur_ref, out_ref, gate, up):
    step = pl.program_id(0)

    @pl.when(step == 0)
    def _():
        gate[...] = jnp.zeros_like(gate)
        up[...] = jnp.zeros_like(up)

    rows = rows_ref[...]
    n = go_ref.shape[1]
    gate[:, :n] += mm(rows, go_ref[...])
    gate[:, n:] += mm(rows, gr_ref[...])
    up[:, :n] += mm(rows, uo_ref[...])
    up[:, n:] += mm(rows, ur_ref[...])

    @pl.when(step == pl.num_programs(0) - 1)
    def _():
        gated = jnp.minimum(gate[...], CLAMP_LIMIT)
        opened = jnp.clip(up[...], -CLAMP_LIMIT, CLAMP_LIMIT)
        out_ref[...] = (
            (opened + 1.0) * gated * jax.nn.sigmoid(SWISH_SLOPE * gated)
        ).astype(BF16)


def hidden_units(rows, go, uo, gr, ur):
    count, width = rows.shape
    n = go.shape[1]
    kb = 1024
    weight = pl.BlockSpec((kb, n), lambda i: (i, 0))
    return pl.pallas_call(
        hidden_kernel,
        grid=(width // kb,),
        in_specs=[pl.BlockSpec((count, kb), lambda i: (0, i)), weight, weight, weight, weight],
        out_specs=pl.BlockSpec((count, 2 * n), lambda i: (0, 0)),
        out_shape=jax.ShapeDtypeStruct((count, 2 * n), BF16),
        scratch_shapes=[pltpu.VMEM((count, 2 * n), F32)] * 2,
        compiler_params=params(),
        name="hidden",
    )(rows, go, uo, gr, ur)


def down_kernel(ho_ref, hp_ref, down_ref, out_ref):
    r = pl.program_id(0)
    n = down_ref.shape[0] // 4
    unit = lambda s: down_ref[pl.ds(pl.multiple_of(s * n, n), n), :]
    near = r + 1 - 2 * (r % 2)
    total = mm(ho_ref[0, :, :n], unit(r)) + mm(ho_ref[0, :, n:], unit(3 - r))
    total += mm(hp_ref[0, :, :n], unit(near)) + mm(hp_ref[0, :, n:], unit(3 - near))
    out_ref[...] = total.astype(BF16).reshape(out_ref.shape)


def down_rows(ho, hp, down):
    sources, rows, both = ho.shape
    cols = down.shape[1]
    near = lambda r: (r + 1 - 2 * (r % 2), 0, 0)
    return pl.pallas_call(
        down_kernel,
        grid=(sources,),
        in_specs=[
            pl.BlockSpec((1, rows, both), lambda r: (r, 0, 0)),
            pl.BlockSpec((1, rows, both), near),
            pl.BlockSpec(down.shape, lambda r: (0, 0)),
        ],
        out_specs=pl.BlockSpec((rows // CAP, 1, CAP, cols), lambda r: (0, r, 0, 0)),
        out_shape=jax.ShapeDtypeStruct((rows // CAP, sources, CAP, cols), BF16),
        compiler_params=params(),
        name="down",
    )(ho, hp, down)


def combine_kernel(res_ref, routes_ref, logits_ref, out_ref):
    experts = res_ref.shape[0]
    first, second, count, before = chosen(routes_ref[0], experts)
    logits = logits_ref[0].astype(F32)
    l0 = jnp.sum(jnp.where(first, logits, 0.0), axis=0, keepdims=True)
    l1 = jnp.sum(jnp.where(second, logits, 0.0), axis=0, keepdims=True)
    w0 = 1.0 / (1.0 + jnp.exp(l1 - l0))
    w1 = 1.0 / (1.0 + jnp.exp(l0 - l1))
    weight = jnp.where(first, w0, 0.0) + jnp.where(second, w1, 0.0)
    place = slot_matrix(weight, before, count)
    coarse = place.astype(BF16)
    fine = (place - coarse.astype(F32)).astype(BF16)
    res = res_ref[...].reshape(experts * CAP, res_ref.shape[3])
    total = mm(coarse, res, ((0,), (0,))) + mm(fine, res, ((0,), (0,)))
    out_ref[...] = total.astype(BF16)


def combined(res, routes, logits):
    experts, blocks, _, cols = res.shape
    toks = routes.shape[2]
    return pl.pallas_call(
        combine_kernel,
        grid=(blocks,),
        in_specs=[
            pl.BlockSpec((experts, 1, CAP, cols), lambda r: (0, r, 0, 0)),
            pl.BlockSpec((1, 2, toks), lambda r: (r, 0, 0)),
            pl.BlockSpec((1, experts, toks), lambda r: (r, 0, 0)),
        ],
        out_specs=pl.BlockSpec((toks, cols), lambda r: (r, 0)),
        out_shape=jax.ShapeDtypeStruct((blocks * toks, cols), BF16),
        compiler_params=params(),
        name="combine",
    )(res, routes, logits)


def per_device(
    mix_input,
    moe_input,
    norm_mix,
    query_weight,
    forget_weight,
    value_weight,
    forget_gap,
    norm_out,
    norm_moe,
    router_weight,
    expert_gate,
    expert_up,
    expert_down,
    routes,
):
    toks, width = moe_input.shape
    experts = router_weight.shape[1]
    x = lax.axis_index("tp").astype(jnp.int32).reshape(1)
    near = [(i, i ^ 1) for i in range(4)]
    far = [(i, 3 - i) for i in range(4)]
    by_block = routes.reshape(4, toks, 2).transpose(0, 2, 1)

    rows_b, logits, own = front(
        x, moe_input, norm_moe.reshape(1, -1), router_weight, by_block, experts
    )
    rows_near = lax.ppermute(rows_b, "tp", near)
    gate_far = lax.ppermute(expert_gate[0], "tp", far)
    up_far = lax.ppermute(expert_up[0], "tp", far)
    swap = lambda a: lax.all_to_all(a, EP, split_axis=0, concat_axis=0, tiled=True)
    own_rows = swap(own).reshape(experts * CAP, width)
    other = refill(x ^ 1, rows_near, by_block, experts)
    near_rows = swap(other).reshape(experts * CAP, width)

    rows_a = normed(mix_input, norm_mix).astype(BF16)
    group_a = lax.all_gather(rows_a, "tp", axis=0, tiled=True)
    group_logits = lax.all_gather(logits, "tp", axis=0).transpose(0, 2, 1)
    inside, query, packed = mixer(
        group_a, query_weight, forget_weight, value_weight, forget_gap.reshape(1, -1)
    )
    state = arriving_state(packed)
    mixer_out = readout(inside, query, state, norm_out.reshape(1, -1))

    weights = (expert_gate[0], expert_up[0], gate_far, up_far)
    h_own = lax.all_gather(hidden_units(own_rows, *weights), "tp", axis=0)
    h_near = lax.all_gather(hidden_units(near_rows, *weights), "tp", axis=0)
    summed = down_rows(h_own, h_near, expert_down[0])
    returned = swap(summed)
    expert_out = combined(returned, by_block, group_logits)
    return (mixer_out, expert_out)


def solution(mesh):
    finer = Mesh(mesh.devices.reshape(4, 4, 2, mesh.shape["tp"]), ("ep_0", "ep_1", "ep_2", "tp"))
    placed = (
        P(EP_TP, None),
        P(EP_TP, None),
        P(),
        P(None, "tp"),
        P(None, "tp"),
        P(None, "tp"),
        P("tp"),
        P("tp"),
        P(),
        P(),
        P(EP, None, "tp"),
        P(EP, None, "tp"),
        P(EP, None, "tp"),
        P(EP, None),
    )
    return jax.shard_map(
        per_device,
        mesh=finer,
        in_specs=placed,
        out_specs=(P(EP, "tp"), P(EP, "tp")),
        check_vma=False,
    )
```

time: 524 us -> 328 us (0.63)
  blocking collectives: 107 us -> 12 us
  other arithmetic: 96.7 us -> 4.57 us
  matrix products: 91.2 us -> 0 us
  Pallas kernels: 0 us -> 74.3 us
  local copies, waits for them, and re-layouts: 66 us -> 3.98 us
  waiting for transfers between devices: 135 us -> 176 us
  starting transfers between devices: 7.35 us -> 40.7 us
    dot_general x32 -> x0, matrix products: 91.2 us -> none  [the longest x8 15.5 us: block_pass(): jnp.einsum('faq,fqp->fap', query_rows * jnp.exp(prefix_log_decay), runnin...]
    pallas_call x0 -> x8, Pallas kernels: none -> 74.3 us  [the longest x1 27.4 us: mixer(): pl.pallas_call(mixer_kernel, grid=(width // kb,), in_specs=[pl.BlockSpec(...]
    ppermute x0 -> x11, waiting for transfers between devices: none -> 70.2 us  [the longest x1 35.2 us: per_device(): up_far = lax.ppermute(expert_up[0], 'tp', far)]
    dot_general x8 -> x0, other arithmetic: 59.1 us -> none  [block_pass(): jnp.einsum('htk,hsk,htsk->hts', query_rows, key_matrix_rows, decays, prec...]
    all_to_all x1 -> x0, blocking collectives: 58.4 us -> none  [per_device(): lax.all_to_all(outgoing, EP, split_axis=0, concat_axis=0, tiled=True)]
    all_gather x5 -> x3, waiting for transfers between devices: 135 us -> 80.6 us  [the longest x1 34.5 us: per_device(): group_a = lax.all_gather(rows_a, 'tp', axis=0, tiled=True)]
    all_gather x4 -> x1, blocking collectives: 48.5 us -> 12 us  [per_device(): group_logits = lax.all_gather(logits, 'tp', axis=0).transpose(0, 2, 1)]
    all_to_all x1 -> x3, waiting for transfers between devices: 0.01 us -> 25 us  [per_device(): lax.all_to_all(a, EP, split_axis=0, concat_axis=0, tiled=True)]
  transfers between devices with their start and end apart: 6 -> 17, of which waited for: 3 -> 13; matrix products, arithmetic and copies ran while one was open for 39% -> 2% of each run, Pallas kernels for 0% -> 19%
where the time goes in v1:
time: 328 us; the launch traced here: 325 us
  waiting for transfers between devices  176 us (54%)
  Pallas kernels  74.3 us (23%)
  starting transfers between devices  40.7 us (12%)
  between operations  14 us (4%)
  blocking collectives  12 us (4%)
  other arithmetic  4.57 us (1%)
  local copies, waits for them, and re-layouts  3.98 us (1%)
    ppermute x1, waiting for transfers between devices, per_device(): up_far = lax.ppermute(expert_up[0], 'tp', far)  35.2 us
    all_gather x1, waiting for transfers between devices, per_device(): group_a = lax.all_gather(rows_a, 'tp', axis=0, tiled=True)  34.5 us
    all_gather x1, waiting for transfers between devices, per_device(): h_near = lax.all_gather(hidden_units(near_rows, *weights), 'tp', axis=0)  32.5 us
    pallas_call x1, Pallas kernels, mixer(): pl.pallas_call(mixer_kernel, grid=(width // kb,), in_specs=[pl.BlockSpec(...  27.4 us
    all_to_all x3, waiting for transfers between devices, per_device(): lax.all_to_all(a, EP, split_axis=0, concat_axis=0, tiled=True)  25 us
    ppermute x1, waiting for transfers between devices, per_device(): rows_near = lax.ppermute(rows_b, 'tp', near)  24.3 us
    all_to_all x3, starting transfers between devices, per_device(): lax.all_to_all(a, EP, split_axis=0, concat_axis=0, tiled=True)  23.8 us
    pallas_call x2, Pallas kernels, hidden_units(): pl.pallas_call(hidden_kernel, grid=(width // kb,), in_specs=[pl.BlockSpec...  17.8 us
  transfers between devices with their start and end apart: 17, of which 13 were waited for; matrix products, arithmetic and copies ran while one was open for 2% of the time, Pallas kernels for 19%

profile of v1, /device:TPU:8, one launch (start us, length us, event | category | flops | bytes accessed | tf_op | source)
XLA Modules:
  0.0 325.4 jit_solution(15815869657964497872)
XLA Ops:
  7.2 2.3 copy.17.router_ref
  9.4 6.2 %front.1 = (bf16[128,4096]{1,0:T(8,128)(2,1)}, bf16[128,32]{1,0:T(8,128)(2,1)}, bf16[32,16,4096]{2,1,0:T(8,128)(2,1)}) custom-call(s32[1]{0:T(128)} %bitcast.15.which, bf16[128,4096]{1,0:T(8,128)(2,1)} %x_ref.1, f32[1,4096]{1,0:T(1,128)} %bitcast.43, bf16[4096,32]{1,0:T(8,128)(2,1)} %copy.17.router_ref, s32[4,2,128]{2,1,0:T(2,128)} %bitcast.40), custom_call_target="tpu_custom_call" | custom-call | tf_op jit(solution)/shard_map/front/pallas_call | solution.py:88
  15.6 8.9 %all-to-all-start = ((bf16[32,16,4096]{2,1,0:T(8,128)(2,1)}), bf16[32,16,4096]{2,1,0:T(8,128)(2,1)}, u32[]{:S(2)}, u32[]{:S(2)}) async-start(bf16[32,16,4096]{2,1,0:T(8,128)(2,1)} %get-tuple-element.11), calls=%async_computation | async-start | bytes 8388608 | tf_op jit(solution)/shard_map/all_to_all | solution.py:421
  24.5 2.8 collective-permute-start.8
  27.4 0.5 collective-permute-start.9
  27.8 0.3 collective-permute-start.10
  28.1 24.3 %collective-permute-done.10.rows_ref = bf16[128,4096]{1,0:T(8,128)(2,1)S(1)} collective-permute-done((bf16[128,4096]{1,0:T(8,128)(2,1)S(1)}, bf16[128,4096]{1,0:T(8,128)(2,1)S(1)}, u32[]{:S(2)}, u32[]{:S(2)}) %collective-permute-start.10) | collective-permute-done | bytes 1048608 | tf_op jit(solution)/shard_map/ppermute | solution.py:418
  52.5 1.0 copy-done.2
  53.4 4.9 %refill.1 = bf16[32,16,4096]{2,1,0:T(8,128)(2,1)} custom-call(s32[1]{0:T(128)S(6)} %xor.3.which, bf16[128,4096]{1,0:T(8,128)(2,1)} %copy-done.2, s32[4,2,128]{2,1,0:T(2,128)} %bitcast.41), custom_call_target="tpu_custom_call" | custom-call | tf_op jit(solution)/shard_map/refill/pallas_call | solution.py:120
  58.3 17.6 %all-to-all-done = bf16[32,16,4096]{2,1,0:T(8,128)(2,1)} async-done(((bf16[32,16,4096]{2,1,0:T(8,128)(2,1)}), bf16[32,16,4096]{2,1,0:T(8,128)(2,1)}, u32[]{:S(2)}, u32[]{:S(2)}) %all-to-all-start) | async-done | bytes 4194336 | tf_op jit(solution)/shard_map/all_to_all | solution.py:421
  75.9 7.3 %all-to-all-start.1 = ((bf16[32,16,4096]{2,1,0:T(8,128)(2,1)}), bf16[32,16,4096]{2,1,0:T(8,128)(2,1)}, u32[]{:S(2)}, u32[]{:S(2)}) async-start(bf16[32,16,4096]{2,1,0:T(8,128)(2,1)} %refill.1), calls=%async_computation.1 | async-start | bytes 8388608 | tf_op jit(solution)/shard_map/all_to_all | solution.py:421
  83.2 0.0 all-gather.9.cloned.1.call-start
  83.3 35.2 %collective-permute-done.9.ur_ref = bf16[4096,256]{1,0:T(8,128)(2,1)} collective-permute-done((bf16[4096,256]{1,0:T(8,128)(2,1)}, bf16[4096,256]{1,0:T(8,128)(2,1)}, u32[]{:S(2)}, u32[]{:S(2)}) %collective-permute-start.9) | collective-permute-done | bytes 2097184 | tf_op jit(solution)/shard_map/ppermute | solution.py:420
  118.5 8.8 %hidden.2 = bf16[512,512]{1,0:T(8,128)(2,1)} custom-call(bf16[512,4096]{1,0:T(8,128)(2,1)} %bitcast.19.rows_ref, bf16[4096,256]{1,0:T(8,128)(2,1)} %bitcast.29, bf16[4096,256]{1,0:T(8,128)(2,1)} %bitcast.33, bf16[4096,256]{1,0:T(8,128)(2,1)} %collective-permute-done.8.gr_ref, bf16[4096,256]{1,0:T(8,128)(2,1)} %collective-permute-done.9.ur_ref), custom_call_target="tpu_custom_call" | custom-call | tf_op jit(solution)/shard_map/hidden/pallas_call | solution.py:316
  127.4 0.0 all-gather.11.cloned.1.call-start
  127.4 7.4 %all-to-all-done.1 = bf16[32,16,4096]{2,1,0:T(8,128)(2,1)} async-done(((bf16[32,16,4096]{2,1,0:T(8,128)(2,1)}), bf16[32,16,4096]{2,1,0:T(8,128)(2,1)}, u32[]{:S(2)}, u32[]{:S(2)}) %all-to-all-start.1) | async-done | bytes 4194336 | tf_op jit(solution)/shard_map/all_to_all | solution.py:421
  134.8 9.0 %hidden.3 = bf16[512,512]{1,0:T(8,128)(2,1)} custom-call(bf16[512,4096]{1,0:T(8,128)(2,1)} %bitcast.24.rows_ref, bf16[4096,256]{1,0:T(8,128)(2,1)} %bitcast.30, bf16[4096,256]{1,0:T(8,128)(2,1)} %bitcast.34, bf16[4096,256]{1,0:T(8,128)(2,1)} %collective-permute-done.8.gr_ref, bf16[4096,256]{1,0:T(8,128)(2,1)} %collective-permute-done.9.ur_ref), custom_call_target="tpu_custom_call" | custom-call | tf_op jit(solution)/shard_map/hidden/pallas_call | solution.py:316
  143.8 0.0 all-gather.7.cloned.1.call-start
  143.8 0.3 fusion
  144.1 1.3 fusion.2
  145.5 13.7 %all-gather.9.cloned.1.call-done = bf16[2048,512]{1,0:T(8,128)(2,1)} async-done(((bf16[512,512]{1,0:T(8,128)(2,1)}), bf16[2048,512]{1,0:T(8,128)(2,1)}) %all-gather.9.cloned.1.call-update) | async-done | bytes 2097168 | tf_op jit(solution)/shard_map/all_gather | solution.py:436
  159.1 32.5 %all-gather.11.cloned.1.call-done = bf16[2048,512]{1,0:T(8,128)(2,1)} async-done(((bf16[512,512]{1,0:T(8,128)(2,1)}), bf16[2048,512]{1,0:T(8,128)(2,1)}) %all-gather.11.cloned.1.call-update) | async-done | bytes 2097168 | tf_op jit(solution)/shard_map/all_gather | solution.py:437
  191.6 8.4 %down.1 = bf16[32,4,16,1024]{3,2,1,0:T(8,128)(2,1)} custom-call(bf16[4,512,512]{2,1,0:T(8,128)(2,1)} %bitcast.36, bf16[4,512,512]{2,1,0:T(8,128)(2,1)} %bitcast.37, bf16[1024,1024]{1,0:T(8,128)(2,1)} %bitcast.35), custom_call_target="tpu_custom_call" | custom-call | tf_op jit(solution)/shard_map/down/pallas_call | solution.py:342
  200.0 7.6 %all-to-all-start.2 = ((bf16[32,4,16,1024]{3,2,1,0:T(8,128)(2,1)}), bf16[32,4,16,1024]{3,2,1,0:T(8,128)(2,1)}, u32[]{:S(2)}, u32[]{:S(2)}) async-start(bf16[32,4,16,1024]{3,2,1,0:T(8,128)(2,1)} %down.1), calls=%async_computation.2 | async-start | bytes 8388608 | tf_op jit(solution)/shard_map/all_to_all | solution.py:421
  207.6 34.5 %all-gather.7.cloned.1.call-done.a_ref = bf16[512,4096]{1,0:T(8,128)(2,1)} async-done(((bf16[128,4096]{1,0:T(8,128)(2,1)}), bf16[512,4096]{1,0:T(8,128)(2,1)}) %all-gather.7.cloned.1.call-update) | async-done | bytes 4194320 | tf_op jit(solution)/shard_map/all_gather | solution.py:427
  242.1 27.4 %mixer.1 = (f32[512,512]{1,0:T(8,128)}, f32[512,512]{1,0:T(8,128)}, f32[4,136,128]{2,1,0:T(8,128)}) custom-call(bf16[512,4096]{1,0:T(8,128)(2,1)} %all-gather.7.cloned.1.call-done.a_ref, bf16[4096,512]{1,0:T(8,128)(2,1)} %q_ref.1, bf16[4096,512]{1,0:T(8,128)(2,1)} %f_ref.1, bf16[4096,512]{1,0:T(8,128)(2,1)} %v_ref.1, f32[1,512]{1,0:T(1,128)} %bitcast.59), custom_call_target="tpu_custom_call" | custom-call | tf_op jit(solution)/shard_map/mixer/pallas_call | solution.py:184
  269.5 1.8 collective-permute-done
  271.3 0.9 dynamic-slice_select_fusion
  272.2 1.0 broadcast_select_fusion
  273.3 1.6 collective-permute-start.3
  274.8 1.1 collective-permute-start.2
  276.0 2.1 collective-permute-start.1
  278.1 1.1 collective-permute-done.3
  279.2 3.2 collective-permute-done.2
  282.5 0.7 collective-permute-done.1
  283.2 0.1 add_add_fusion
  283.3 5.1 %collective-permute-start.5 = (f32[2,136,128]{2,1,0:T(8,128)S(1)}, f32[2,136,128]{2,1,0:T(8,128)S(1)}, u32[]{:S(2)}, u32[]{:S(2)}) collective-permute-start(f32[2,136,128]{2,1,0:T(8,128)S(1)} %pad_maximum_fusion.2), channel_id=1, source_target_pairs={{0,64},{32,96},{1,65},{33,97},{2,66},{34,98},{3,67},{35,99},{4,68}... | collective-permute-start | bytes 417800 | tf_op jit(solution)/shard_map/ppermute | solution.py:276
  288.4 12.0 %all-gather.2 = bf16[512,32]{1,0:T(8,128)(2,1)S(1)} all-gather(bf16[128,32]{1,0:T(8,128)(2,1)S(1)} %copy-done.3), channel_id=4, replica_groups=mesh['ep_0'=4,'ep_1'=4,'ep_2'=2,'tp'=4] {'tp'}, dimensions={0}, use_global_device_ids=true | all-gather | bytes 40960 | tf_op jit(solution)/shard_map/all_gather | solution.py:428
  300.4 0.7 copy.19
  301.1 1.3 collective-permute-start.6
  302.4 1.9 collective-permute-start.4
  304.4 2.5 collective-permute-done.4
  306.9 0.1 fusion.5
  307.0 0.1 collective-permute-start.7
  307.1 1.3 collective-permute-done.7
  308.5 0.8 fusion.3.state_ref
  309.2 4.4 %readout.1 = bf16[512,512]{1,0:T(8,128)(2,1)} custom-call(f32[512,512]{1,0:T(8,128)} %get-tuple-element.8.inside_ref, f32[512,512]{1,0:T(8,128)} %get-tuple-element.9.query_ref, f32[4,128,128]{2,1,0:T(8,128)} %fusion.3.state_ref, f32[1,512]{1,0:T(1,128)} %bitcast.60), custom_call_target="tpu_custom_call" | custom-call | tf_op jit(solution)/shard_map/readout/pallas_call | solution.py:218
  313.6 5.3 %combine.1 = bf16[512,1024]{1,0:T(8,128)(2,1)} custom-call(bf16[32,4,16,1024]{3,2,1,0:T(8,128)(2,1)} %all-to-all-done.2.res_ref, s32[4,2,128]{2,1,0:T(2,128)} %bitcast.42, bf16[4,32,128]{2,1,0:T(8,128)(2,1)} %bitcast.39), custom_call_target="tpu_custom_call" | custom-call | tf_op jit(solution)/shard_map/combine/pallas_call | solution.py:377
  (32 shorter events, 0.3 us)
Async XLA Ops:
  15.6 8.9 %copy-start = (bf16[1,4096,256]{2,1,0:T(8,128)(2,1)S(1)}, bf16[1,4096,256]{2,1,0:T(8,128)(2,1)}, u32[]{:S(2)}) copy-start(bf16[1,4096,256]{2,1,0:T(8,128)(2,1)} %param.24) | copy-start | bytes 6291460
  15.6 12.2 %copy-start.5 = (bf16[128,4096]{1,0:T(8,128)(2,1)S(1)}, bf16[128,4096]{1,0:T(8,128)(2,1)}, u32[]{:S(2)}) copy-start(bf16[128,4096]{1,0:T(8,128)(2,1)} %get-tuple-element.12) | copy-start | bytes 3145732
  15.6 60.3 %all-to-all-start = ((bf16[32,16,4096]{2,1,0:T(8,128)(2,1)}), bf16[32,16,4096]{2,1,0:T(8,128)(2,1)}, u32[]{:S(2)}, u32[]{:S(2)}) async-start(bf16[32,16,4096]{2,1,0:T(8,128)(2,1)} %get-tuple-element.11), calls=%async_computation | async-start | bytes 8388608 | tf_op jit(solution)/shard_map/all_to_all | solution.py:421
  24.5 58.8 %collective-permute-start.8 = (bf16[4096,256]{1,0:T(8,128)(2,1)S(1)}, bf16[4096,256]{1,0:T(8,128)(2,1)}, u32[]{:S(2)}, u32[]{:S(2)}) collective-permute-start(bf16[4096,256]{1,0:T(8,128)(2,1)S(1)} %bitcast.31), channel_id=1, source_target_pairs={{0,3},{1,2},{2,1},{3,0},{4,7},{5,6},{6,5},{7,4},{8,11},{9,10},{10,... | collective-permute-start | bytes 6291464 | tf_op jit(solution)/shard_map/ppermute | solution.py:419
  27.4 91.1 %collective-permute-start.9 = (bf16[4096,256]{1,0:T(8,128)(2,1)}, bf16[4096,256]{1,0:T(8,128)(2,1)}, u32[]{:S(2)}, u32[]{:S(2)}) collective-permute-start(bf16[4096,256]{1,0:T(8,128)(2,1)} %bitcast.32), channel_id=1, source_target_pairs={{0,3},{1,2},{2,1},{3,0},{4,7},{5,6},{6,5},{7,4},{8,11},{9,10},{10,... | collective-permute-start | bytes 6291464 | tf_op jit(solution)/shard_map/ppermute | solution.py:420
  27.8 24.6 %collective-permute-start.10 = (bf16[128,4096]{1,0:T(8,128)(2,1)S(1)}, bf16[128,4096]{1,0:T(8,128)(2,1)S(1)}, u32[]{:S(2)}, u32[]{:S(2)}) collective-permute-start(bf16[128,4096]{1,0:T(8,128)(2,1)S(1)} %copy-done.5), channel_id=1, source_target_pairs={{0,1},{1,0},{2,3},{3,2},{4,5},{5,4},{6,7},{7,6},{8,9},{9,8},{10,11... | collective-permute-start | bytes 3145736 | tf_op jit(solution)/shard_map/ppermute | solution.py:418
  52.5 1.0 copy-start.2
  75.9 58.8 %all-to-all-start.1 = ((bf16[32,16,4096]{2,1,0:T(8,128)(2,1)}), bf16[32,16,4096]{2,1,0:T(8,128)(2,1)}, u32[]{:S(2)}, u32[]{:S(2)}) async-start(bf16[32,16,4096]{2,1,0:T(8,128)(2,1)} %refill.1), calls=%async_computation.1 | async-start | bytes 8388608 | tf_op jit(solution)/shard_map/all_to_all | solution.py:421
  83.2 75.9 %all-gather.9.cloned.1.call-start = ((), (), s32[]{:S(2)}) async-start(), calls=%async_computation.4 | async-start | bytes 2621440 | tf_op jit(solution)/shard_map/all_gather | solution.py:436
  127.4 64.2 %all-gather.11.cloned.1.call-start = ((), (), s32[]{:S(2)}) async-start(), calls=%async_computation.5 | async-start | bytes 2621440 | tf_op jit(solution)/shard_map/all_gather | solution.py:437
  134.8 9.1 %copy-start.1 = (bf16[128,4096]{1,0:T(8,128)(2,1)S(1)}, bf16[128,4096]{1,0:T(8,128)(2,1)}, u32[]{:S(2)}) copy-start(bf16[128,4096]{1,0:T(8,128)(2,1)} %param.14) | copy-start | bytes 3145732
  134.8 9.4 %copy-start.4 = (f32[4096]{0:T(1024)S(1)}, f32[4096]{0:T(1024)}, u32[]{:S(2)}) copy-start(f32[4096]{0:T(1024)} %param.16) | copy-start | bytes 49156
  143.8 98.3 %all-gather.7.cloned.1.call-start = ((), (), s32[]{:S(2)}) async-start(), calls=%async_computation.3 | async-start | bytes 5242880 | tf_op jit(solution)/shard_map/all_gather | solution.py:427
  200.0 113.6 %all-to-all-start.2 = ((bf16[32,4,16,1024]{3,2,1,0:T(8,128)(2,1)}), bf16[32,4,16,1024]{3,2,1,0:T(8,128)(2,1)}, u32[]{:S(2)}, u32[]{:S(2)}) async-start(bf16[32,4,16,1024]{3,2,1,0:T(8,128)(2,1)} %down.1), calls=%async_computation.2 | async-start | bytes 8388608 | tf_op jit(solution)/shard_map/all_to_all | solution.py:421
  269.5 18.9 %copy-start.3 = (bf16[128,32]{1,0:T(8,128)(2,1)S(1)}, bf16[128,32]{1,0:T(8,128)(2,1)}, u32[]{:S(2)}) copy-start(bf16[128,32]{1,0:T(8,128)(2,1)} %get-tuple-element.13) | copy-start | bytes 24580
  269.5 1.8 collective-permute-start
  273.3 6.0 %collective-permute-start.3 = (f32[2,136,128]{2,1,0:T(8,128)S(1)}, f32[2,136,128]{2,1,0:T(8,128)S(1)}, u32[]{:S(2)}, u32[]{:S(2)}) collective-permute-start(f32[2,136,128]{2,1,0:T(8,128)S(1)} %pad_maximum_fusion.1), channel_id=1, source_target_pairs={{0,8},{8,16},{16,24},{24,0},{1,9},{9,17},{17,25},{25,1},{2,10},{10... | collective-permute-start | bytes 417800 | tf_op jit(solution)/shard_map/ppermute | solution.py:267
  274.8 7.6 %collective-permute-start.2 = (f32[2,136,128]{2,1,0:T(8,128)S(1)}, f32[2,136,128]{2,1,0:T(8,128)S(1)}, u32[]{:S(2)}, u32[]{:S(2)}) collective-permute-start(f32[2,136,128]{2,1,0:T(8,128)S(1)} %pad_maximum_fusion.1), channel_id=1, source_target_pairs={{0,16},{8,24},{16,0},{24,8},{1,17},{9,25},{17,1},{25,9},{2,18},{10... | collective-permute-start | bytes 417800 | tf_op jit(solution)/shard_map/ppermute | solution.py:267
  276.0 7.2 %collective-permute-start.1 = (f32[2,136,128]{2,1,0:T(8,128)S(1)}, f32[2,136,128]{2,1,0:T(8,128)S(1)}, u32[]{:S(2)}, u32[]{:S(2)}) collective-permute-start(f32[2,136,128]{2,1,0:T(8,128)S(1)} %pad_maximum_fusion.1), channel_id=1, source_target_pairs={{0,24},{8,0},{16,8},{24,16},{1,25},{9,1},{17,9},{25,17},{2,26},{10... | collective-permute-start | bytes 417800 | tf_op jit(solution)/shard_map/ppermute | solution.py:267
  283.3 21.0 %collective-permute-start.5 = (f32[2,136,128]{2,1,0:T(8,128)S(1)}, f32[2,136,128]{2,1,0:T(8,128)S(1)}, u32[]{:S(2)}, u32[]{:S(2)}) collective-permute-start(f32[2,136,128]{2,1,0:T(8,128)S(1)} %pad_maximum_fusion.2), channel_id=1, source_target_pairs={{0,64},{32,96},{1,65},{33,97},{2,66},{34,98},{3,67},{35,99},{4,68}... | collective-permute-start | bytes 417800 | tf_op jit(solution)/shard_map/ppermute | solution.py:276
  301.1 5.8 %collective-permute-start.6 = (f32[2,136,128]{2,1,0:T(8,128)S(1)}, f32[2,136,128]{2,1,0:T(8,128)S(1)}, u32[]{:S(2)}, u32[]{:S(2)}) collective-permute-start(f32[2,136,128]{2,1,0:T(8,128)S(1)} %pad_maximum_fusion.2), channel_id=1, source_target_pairs={{0,96},{1,97},{2,98},{3,99},{4,100},{5,101},{6,102},{7,103},{8,104... | collective-permute-start | bytes 417800 | tf_op jit(solution)/shard_map/ppermute | solution.py:276
  302.4 4.5 %collective-permute-start.4 = (f32[2,136,128]{2,1,0:T(8,128)S(1)}, f32[2,136,128]{2,1,0:T(8,128)S(1)}, u32[]{:S(2)}, u32[]{:S(2)}) collective-permute-start(f32[2,136,128]{2,1,0:T(8,128)S(1)} %pad_maximum_fusion.2), channel_id=1, source_target_pairs={{0,32},{32,64},{64,96},{1,33},{33,65},{65,97},{2,34},{34,66},{66,9... | collective-permute-start | bytes 417800 | tf_op jit(solution)/shard_map/ppermute | solution.py:276
  307.0 1.4 collective-permute-start.7
Sparse Core Ops, SparseCore 0:
  127.5 31.5 all-gather.8
  160.8 30.7 all-gather.10
  193.8 48.1 all-gather.6

commit v2 on v1

v2 whole, which is shorter than its diff:
```python
import functools

import jax
import jax.numpy as jnp
from jax import lax
from jax.experimental import pallas as pl
from jax.experimental.pallas import tpu as pltpu
from jax.sharding import Mesh
from jax.sharding import PartitionSpec as P

HEAD_DIM = 128
HALF = 8
EP = ("ep_0", "ep_1", "ep_2")
EP_TP = ("ep_0", "ep_1", "ep_2", "tp")

EPSILON = 1e-06
CLAMP_LIMIT = 7.0
SWISH_SLOPE = 1.702
EXACT = lax.Precision.HIGHEST
F32 = jnp.float32
BF16 = jnp.bfloat16


def mm(a, b, contract=((1,), (0,)), precision=None):
    return lax.dot_general(
        a, b, (contract, ((), ())), precision=precision, preferred_element_type=F32
    )


def params(mib=56, axes=("arbitrary",)):
    return pltpu.CompilerParams(vmem_limit_bytes=mib << 20, dimension_semantics=axes)


def normed(row_data, gain_vec):
    as_float = row_data.astype(F32)
    scale = lax.rsqrt(jnp.mean(as_float * as_float, axis=-1, keepdims=True) + EPSILON)
    return as_float * scale * gain_vec


def chosen(routes, experts):
    toks = routes.shape[1]
    ids = lax.broadcasted_iota(jnp.int32, (experts, toks), 0)
    first = routes[0:1, :] == ids
    second = routes[1:2, :] == ids
    count = jnp.where(first | second, 1.0, 0.0)
    earlier = (
        lax.broadcasted_iota(jnp.int32, (toks, toks), 0)
        < lax.broadcasted_iota(jnp.int32, (toks, toks), 1)
    )
    before = mm(count.astype(BF16), jnp.where(earlier, 1.0, 0.0).astype(BF16))
    return first, second, count, before


def slot_matrix(weight, before, count, half):
    experts, toks = weight.shape
    place = lax.broadcasted_iota(jnp.int32, (experts, HALF, toks), 1) + half * HALF
    here = (before[:, None, :] == place.astype(F32)) & (count[:, None, :] > 0.5)
    return jnp.where(here, weight[:, None, :], 0.0).reshape(experts * HALF, toks)


def fill(routes, rows, experts):
    _, _, count, before = chosen(routes, experts)
    pick = lambda half: slot_matrix(count, before, count, half).astype(BF16)
    return [mm(pick(half), rows).astype(BF16) for half in range(2)]


def front_kernel(src, x_ref, gain_ref, router_ref, routes_ref, rows_ref, logits_ref, buf_ref, *, group):
    step = pl.program_id(0)
    width = x_ref.shape[1]

    @pl.when(step == 0)
    def _():
        rows_ref[...] = normed(x_ref[...], gain_ref[...]).astype(BF16)
        logits_ref[...] = mm(router_ref[...], rows_ref[...], ((1,), (1,))).astype(BF16)

    low, high = fill(routes_ref[0] - step * group, rows_ref[...], group)
    buf_ref[:, :width] = low
    buf_ref[:, width:] = high


def refill_kernel(src, rows_ref, router_ref, routes_ref, logits_ref, low_ref, high_ref, *, group):
    step = pl.program_id(0)

    @pl.when(step == 0)
    def _():
        logits_ref[...] = mm(router_ref[...], rows_ref[...], ((1,), (1,))).astype(BF16)

    low_ref[...], high_ref[...] = fill(routes_ref[0] - step * group, rows_ref[...], group)


def front(src, x, gain, router, routes):
    toks, width = x.shape
    experts = router.shape[0]
    group = 8
    whole = lambda i, s: (0, 0)
    return pl.pallas_call(
        functools.partial(front_kernel, group=group),
        grid_spec=pltpu.PrefetchScalarGridSpec(
            num_scalar_prefetch=1,
            grid=(experts // group,),
            in_specs=[
                pl.BlockSpec((toks, width), whole),
                pl.BlockSpec((1, width), whole),
                pl.BlockSpec(router.shape, whole),
                pl.BlockSpec((1, 2, toks), lambda i, s: (s[0], 0, 0)),
            ],
            out_specs=[
                pl.BlockSpec((toks, width), whole),
                pl.BlockSpec((experts, toks), whole),
                pl.BlockSpec((group * HALF, 2 * width), lambda i, s: (i, 0)),
            ],
        ),
        out_shape=[
            jax.ShapeDtypeStruct((toks, width), BF16),
            jax.ShapeDtypeStruct((experts, toks), BF16),
            jax.ShapeDtypeStruct((experts * HALF, 2 * width), BF16),
        ],
        compiler_params=params(),
        name="front",
    )(src, x, gain, router, routes)


def refill(src, rows, router, routes):
    toks, width = rows.shape
    experts = router.shape[0]
    group = 8
    whole = lambda i, s: (0, 0)
    return pl.pallas_call(
        functools.partial(refill_kernel, group=group),
        grid_spec=pltpu.PrefetchScalarGridSpec(
            num_scalar_prefetch=1,
            grid=(experts // group,),
            in_specs=[
                pl.BlockSpec((toks, width), whole),
                pl.BlockSpec(router.shape, whole),
                pl.BlockSpec((1, 2, toks), lambda i, s: (s[1], 0, 0)),
            ],
            out_specs=[
                pl.BlockSpec((experts, toks), whole),
                pl.BlockSpec((group * HALF, width), lambda i, s: (i, 0)),
                pl.BlockSpec((group * HALF, width), lambda i, s: (i, 0)),
            ],
        ),
        out_shape=[
            jax.ShapeDtypeStruct((experts, toks), BF16),
            jax.ShapeDtypeStruct((experts * HALF, width), BF16),
            jax.ShapeDtypeStruct((experts * HALF, width), BF16),
        ],
        compiler_params=params(),
        name="refill",
    )(src, rows, router, routes)


def mixer_kernel(
    src, a0, a1, a2, a3, q_ref, f_ref, v_ref, gap_ref, inside_ref, query_ref, packed_ref, qa, fa, va, group
):
    step = pl.program_id(0)

    @pl.when(step == 0)
    def _():
        qa[...] = jnp.zeros_like(qa)
        fa[...] = jnp.zeros_like(fa)
        va[...] = jnp.zeros_like(va)

    toks = a0.shape[0]
    for k, part in enumerate((a0, a1, a2, a3)):
        group[pl.ds(pl.multiple_of(src[k] * toks, toks), toks), :] = part[...]
    a = group[...]
    qa[...] += mm(a, q_ref[...])
    fa[...] += mm(a, f_ref[...])
    va[...] += mm(a, v_ref[...])

    @pl.when(step == pl.num_programs(0) - 1)
    def _():
        rows = a.shape[0]
        causal = (
            lax.broadcasted_iota(jnp.int32, (rows, rows), 0)
            >= lax.broadcasted_iota(jnp.int32, (rows, rows), 1)
        )
        ones = jnp.where(causal, 1.0, 0.0)
        heads = packed_ref.shape[0]
        for h in range(heads):
            at = slice(h * HEAD_DIM, (h + 1) * HEAD_DIM)
            shut = gap_ref[:, at] * jax.nn.sigmoid(-fa[:, at])
            sums = mm(ones, jnp.log1p(-shut), precision=EXACT)
            last = sums[rows - 1 :, :]
            value = va[:, at]
            query = qa[:, at] * jnp.exp(sums)
            scores = mm(query, shut * jnp.exp(-sums), ((1,), (1,)), EXACT)
            scores = jnp.where(causal, scores, 0.0)
            inside_ref[:, at] = mm(scores, value, precision=EXACT)
            query_ref[:, at] = query
            packed_ref[h, :HEAD_DIM, :] = mm(
                value, shut * jnp.exp(last - sums), ((0,), (0,)), EXACT
            )
            packed_ref[h, HEAD_DIM:, :] = jnp.broadcast_to(last, (8, HEAD_DIM))


def mixer(src, parts, wq, wf, wv, gap):
    toks, width = parts[0].shape
    rows = 4 * toks
    cols = wq.shape[1]
    heads = cols // HEAD_DIM
    kb = 512
    fixed = lambda i, s: (0, 0)
    weight = pl.BlockSpec((kb, cols), lambda i, s: (i, 0))
    return pl.pallas_call(
        mixer_kernel,
        grid_spec=pltpu.PrefetchScalarGridSpec(
            num_scalar_prefetch=1,
            grid=(width // kb,),
            in_specs=[pl.BlockSpec((toks, kb), lambda i, s: (0, i))] * 4
            + [weight, weight, weight, pl.BlockSpec((1, cols), fixed)],
            out_specs=[
                pl.BlockSpec((rows, cols), fixed),
                pl.BlockSpec((rows, cols), fixed),
                pl.BlockSpec((heads, HEAD_DIM + 8, HEAD_DIM), lambda i, s: (0, 0, 0)),
            ],
            scratch_shapes=[pltpu.VMEM((rows, cols), F32)] * 3 + [pltpu.VMEM((rows, kb), BF16)],
        ),
        out_shape=[
            jax.ShapeDtypeStruct((rows, cols), F32),
            jax.ShapeDtypeStruct((rows, cols), F32),
            jax.ShapeDtypeStruct((heads, HEAD_DIM + 8, HEAD_DIM), F32),
        ],
        compiler_params=params(),
        name="mixer",
    )(src, *parts, wq, wf, wv, gap)


def readout_kernel(inside_ref, query_ref, state_ref, gain_ref, out_ref):
    total = inside_ref[...] + mm(query_ref[...], state_ref[0], ((1,), (1,)), EXACT)
    out_ref[...] = normed(total, gain_ref[...]).astype(BF16)


def readout(inside, query, state, gain):
    rows, cols = inside.shape
    block = pl.BlockSpec((rows, HEAD_DIM), lambda h: (0, h))
    return pl.pallas_call(
        readout_kernel,
        grid=(cols // HEAD_DIM,),
        in_specs=[
            block,
            block,
            pl.BlockSpec((1, HEAD_DIM, HEAD_DIM), lambda h: (h, 0, 0)),
            pl.BlockSpec((1, HEAD_DIM), lambda h: (0, h)),
        ],
        out_specs=block,
        out_shape=jax.ShapeDtypeStruct((rows, cols), BF16),
        compiler_params=params(),
        name="readout",
    )(inside, query, state, gain)


def pieces(packed):
    return packed[:, HEAD_DIM : HEAD_DIM + 1, :], packed[:, :HEAD_DIM, :]


def link(earlier, later):
    return earlier[0] + later[0], jnp.exp(later[0]) * earlier[1] + later[1]


def pack(part):
    heads = part[1].shape[0]
    return jnp.concatenate(
        [part[1], jnp.broadcast_to(part[0], (heads, 8, HEAD_DIM))], axis=1
    )


def masked(flag, part):
    return jax.tree.map(lambda a: jnp.where(flag, a, 0.0), part)


def arriving_state(packed):
    core = lax.axis_index("ep_2")
    row = lax.axis_index("ep_1")
    other = lax.ppermute(packed, "ep_2", [(0, 1), (1, 0)])
    is_second = core == 1
    low = jnp.where(is_second, other, packed)
    high = jnp.where(is_second, packed, other)
    half = packed.shape[0] // 2
    mine = lambda a: lax.dynamic_slice_in_dim(a, core * half, half, 0)
    chip = link(pieces(mine(low)), pieces(mine(high)))
    count = lax.axis_size("ep_1")
    sent = pack(chip)
    before = after = None
    for d in range(count - 1, 0, -1):
        came = pieces(lax.ppermute(sent, "ep_1", [(i, (i + d) % count) for i in range(count)]))
        early = masked(row >= d, came)
        late = masked(row < d, came)
        before = early if before is None else link(before, early)
        after = late if after is None else link(after, late)
    plane = pack(link(link(before, chip), after))
    planes = None
    count = lax.axis_size("ep_0")
    for d in range(count - 1, 0, -1):
        came = pieces(lax.ppermute(plane, "ep_0", [(i, i + d) for i in range(count - d)]))
        planes = came if planes is None else link(planes, came)
    state = link(planes, before)[1]
    swapped = lax.ppermute(state, "ep_2", [(0, 1), (1, 0)])
    entering = jnp.concatenate(
        [jnp.where(is_second, swapped, state), jnp.where(is_second, state, swapped)], axis=0
    )
    first_core = pieces(low)
    return jnp.where(is_second, jnp.exp(first_core[0]) * entering + first_core[1], entering)


def hidden_kernel(own_ref, near_ref, go_ref, uo_ref, gf_ref, uf_ref, out_ref, gate, up):
    step = pl.program_id(0)

    @pl.when(step == 0)
    def _():
        gate[...] = jnp.zeros_like(gate)
        up[...] = jnp.zeros_like(up)

    rows = jnp.concatenate([own_ref[...], near_ref[...]], axis=0)
    n = go_ref.shape[1]
    gate[:, :n] += mm(rows, go_ref[...])
    gate[:, n:] += mm(rows, gf_ref[...])
    up[:, :n] += mm(rows, uo_ref[...])
    up[:, n:] += mm(rows, uf_ref[...])

    @pl.when(step == pl.num_programs(0) - 1)
    def _():
        gated = jnp.minimum(gate[...], CLAMP_LIMIT)
        opened = jnp.clip(up[...], -CLAMP_LIMIT, CLAMP_LIMIT)
        out_ref[...] = (
            (opened + 1.0) * gated * jax.nn.sigmoid(SWISH_SLOPE * gated)
        ).astype(BF16)


def hidden_units(own, near, half, weights):
    count = own.shape[0]
    width, n = weights[0].shape
    kb = 1024
    weight = pl.BlockSpec((kb, n), lambda i: (i, 0))
    return pl.pallas_call(
        hidden_kernel,
        grid=(width // kb,),
        in_specs=[
            pl.BlockSpec((count, kb), lambda i: (0, i + half * (width // kb))),
            pl.BlockSpec((count, kb), lambda i: (0, i)),
            weight,
            weight,
            weight,
            weight,
        ],
        out_specs=pl.BlockSpec((2 * count, 2 * n), lambda i: (0, 0)),
        out_shape=jax.ShapeDtypeStruct((2 * count, 2 * n), BF16),
        scratch_shapes=[pltpu.VMEM((2 * count, 2 * n), F32)] * 2,
        compiler_params=params(),
        name="hidden",
    )(own, near, *weights)


def down_kernel(src, h_own, h_near, h_far, h_opp, down_ref, out_ref):
    k = pl.program_id(0)
    n = down_ref.shape[0] // 4
    rows = out_ref.shape[0]
    unit = lambda s: down_ref[pl.ds(pl.multiple_of(s * n, n), n), :]
    for this, (mine, other, twin) in enumerate(
        ((h_own, h_near, 1), (h_near, h_own, 0), (h_far, h_opp, 3), (h_opp, h_far, 2))
    ):

        @pl.when(k == this)
        def _():
            s, t = src[this], src[twin]
            total = mm(mine[:rows, :n], unit(s)) + mm(mine[:rows, n:], unit(3 - s))
            total += mm(other[rows:, :n], unit(t)) + mm(other[rows:, n:], unit(3 - t))
            out_ref[...] = total.astype(BF16)


def down_rows(src, parts, down):
    both, width = parts[0].shape
    cols = down.shape[1]
    whole = lambda k, s: (0, 0)
    return pl.pallas_call(
        down_kernel,
        grid_spec=pltpu.PrefetchScalarGridSpec(
            num_scalar_prefetch=1,
            grid=(4,),
            in_specs=[pl.BlockSpec((both, width), whole)] * 4 + [pl.BlockSpec(down.shape, whole)],
            out_specs=pl.BlockSpec((both // 2, cols), lambda k, s: (0, s[k])),
        ),
        out_shape=jax.ShapeDtypeStruct((both // 2, 4 * cols), BF16),
        compiler_params=params(),
        name="down",
    )(src, *parts, down)


def combine_kernel(src, low_ref, high_ref, routes_ref, logits_ref, out_ref):
    experts = logits_ref.shape[1]
    first, second, count, before = chosen(routes_ref[0], experts)
    logits = logits_ref[0].astype(F32)
    l0 = jnp.sum(jnp.where(first, logits, 0.0), axis=0, keepdims=True)
    l1 = jnp.sum(jnp.where(second, logits, 0.0), axis=0, keepdims=True)
    w0 = 1.0 / (1.0 + jnp.exp(l1 - l0))
    w1 = 1.0 / (1.0 + jnp.exp(l0 - l1))
    weight = jnp.where(first, w0, 0.0) + jnp.where(second, w1, 0.0)
    total = None
    for half, res_ref in enumerate((low_ref, high_ref)):
        place = slot_matrix(weight, before, count, half)
        coarse = place.astype(BF16)
        fine = (place - coarse.astype(F32)).astype(BF16)
        res = res_ref[...]
        part = mm(coarse, res, ((0,), (0,))) + mm(fine, res, ((0,), (0,)))
        total = part if total is None else total + part
    out_ref[...] = total.astype(BF16)


def combined(src, low, high, routes, logits):
    slots = low.shape[0]
    cols = low.shape[1] // 4
    toks = routes.shape[2]
    res = pl.BlockSpec((slots, cols), lambda k, s: (0, s[k]))
    return pl.pallas_call(
        combine_kernel,
        grid_spec=pltpu.PrefetchScalarGridSpec(
            num_scalar_prefetch=1,
            grid=(4,),
            in_specs=[
                res,
                res,
                pl.BlockSpec((1, 2, toks), lambda k, s: (s[k], 0, 0)),
                pl.BlockSpec((1,) + logits.shape[1:], lambda k, s: (k, 0, 0)),
            ],
            out_specs=pl.BlockSpec((toks, cols), lambda k, s: (s[k], 0)),
        ),
        out_shape=jax.ShapeDtypeStruct((4 * toks, cols), BF16),
        compiler_params=params(),
        name="combine",
    )(src, low, high, routes, logits)


NEAR = [(i, i ^ 1) for i in range(4)]
FAR = [(i, 3 - i) for i in range(4)]


def to_near(a):
    return lax.ppermute(a, "tp", NEAR)


def to_far(a):
    return lax.ppermute(a, "tp", FAR)


def shared(a):
    far = to_far(a)
    near = to_near(a)
    return a, near, far, to_near(far)


def swap(a):
    experts = 32
    rows, cols = a.shape
    out = lax.all_to_all(
        a.reshape(experts, rows // experts, cols), EP, split_axis=0, concat_axis=0, tiled=True
    )
    return out.reshape(rows, cols)


def per_device(
    mix_input,
    moe_input,
    norm_mix,
    query_weight,
    forget_weight,
    value_weight,
    forget_gap,
    norm_out,
    norm_moe,
    router_weight,
    expert_gate,
    expert_up,
    expert_down,
    routes,
):
    toks = moe_input.shape[0]
    x = lax.axis_index("tp").astype(jnp.int32)
    src = jnp.stack([x, x ^ 1, 3 - x, x ^ 2])
    by_block = routes.reshape(4, toks, 2).transpose(0, 2, 1)
    router = router_weight.T

    gate_far = to_far(expert_gate[0])
    rows_b, logits, own = front(src, moe_input, norm_moe.reshape(1, -1), router, by_block)
    own_rows = swap(own)
    rows_near = to_near(rows_b)
    mix_input, _ = lax.optimization_barrier((mix_input, rows_b))
    rows_a = normed(mix_input, norm_mix).astype(BF16)
    group_a = shared(rows_a)
    up_far = to_far(expert_up[0])
    logits_near, low, high = refill(src, rows_near, router, by_block)
    low, own_rows = lax.optimization_barrier((low, own_rows))
    low_rows = swap(low)
    high, low_rows = lax.optimization_barrier((high, low_rows))
    high_rows = swap(high)
    logits = jnp.stack([logits, logits_near])
    logits = jnp.concatenate([logits, to_far(logits)])

    inside, query, packed = mixer(
        src,
        group_a,
        query_weight,
        forget_weight,
        value_weight,
        forget_gap.reshape(1, -1),
    )

    low_rows, packed = lax.optimization_barrier((low_rows, packed))
    weights = (expert_gate[0], expert_up[0], gate_far, up_far)
    h_low = shared(hidden_units(own_rows, low_rows, 0, weights))
    high_rows, far = lax.optimization_barrier((high_rows, h_low[2]))
    h_high = shared(hidden_units(own_rows, high_rows, 1, weights))
    opp, high_own = lax.optimization_barrier((h_low[3], h_high[0]))
    back_low = swap(down_rows(src, h_low[:2] + (far, opp), expert_down[0]))
    back_high = swap(down_rows(src, (high_own,) + h_high[1:], expert_down[0]))

    state = arriving_state(packed)
    mixer_out = readout(inside, query, state, norm_out.reshape(1, -1))
    expert_out = combined(src, back_low, back_high, by_block, logits)
    return (mixer_out, expert_out)


def solution(mesh):
    finer = Mesh(mesh.devices.reshape(4, 4, 2, mesh.shape["tp"]), ("ep_0", "ep_1", "ep_2", "tp"))
    placed = (
        P(EP_TP, None),
        P(EP_TP, None),
        P(),
        P(None, "tp"),
        P(None, "tp"),
        P(None, "tp"),
        P("tp"),
        P("tp"),
        P(),
        P(),
        P(EP, None, "tp"),
        P(EP, None, "tp"),
        P(EP, None, "tp"),
        P(EP, None),
    )

    return jax.shard_map(
        per_device,
        mesh=finer,
        in_specs=placed,
        out_specs=(P(EP, "tp"), P(EP, "tp")),
        check_vma=False,
    )
```

time: 328 us -> 350 us (1.067)
  starting transfers between devices: 40.7 us -> 69.6 us
  between operations: 14 us -> 1.03 us
  blocking collectives: 12 us -> 0 us
  Pallas kernels: 74.3 us -> 82.6 us
  waiting for transfers between devices: 176 us -> 181 us
  other arithmetic: 4.57 us -> 8.55 us
    all_gather x3 -> x0, waiting for transfers between devices: 80.6 us -> none  [the longest x1 34.5 us: per_device(): group_a = lax.all_gather(rows_a, 'tp', axis=0, tiled=True)]
    ppermute x3 -> x13, waiting for transfers between devices: 59.5 us -> 135 us  [the longest x6 82.5 us: to_far(): return lax.ppermute(a, 'tp', FAR)]
    ppermute x3 -> x13, starting transfers between devices: 3.6 us -> 18.3 us  [the longest x6 14.4 us: to_far(): return lax.ppermute(a, 'tp', FAR)]
    all_to_all x3 -> x5, starting transfers between devices: 23.8 us -> 37.5 us  [swap(): lax.all_to_all(a.reshape(experts, rows // experts, cols), EP, split_axis=...]
    all_gather x1 -> x0, blocking collectives: 12 us -> none  [per_device(): group_logits = lax.all_gather(logits, 'tp', axis=0).transpose(0, 2, 1)]
    ppermute x3, waiting for transfers between devices: 2.55 us -> 14.3 us  [arriving_state(): lax.ppermute(plane, 'ep_0', [(i, i + d) for i in range(count - d)])]
    pallas_call x4 -> x5, Pallas kernels: 45.9 us -> 53.9 us  [the longest x1 28.5 us: mixer(): pl.pallas_call(mixer_kernel, grid_spec=pltpu.PrefetchScalarGridSpec(num_s...]
    ppermute x3, waiting for transfers between devices: 5.05 us -> 10.9 us  [arriving_state(): lax.ppermute(sent, 'ep_1', [(i, (i + d) % count) for i in range(count)])]
  transfers between devices with their start and end apart: 17 -> 26, of which waited for: 13 -> 17; matrix products, arithmetic and copies ran while one was open for 2% -> 2% of each run, Pallas kernels for 19% -> 18%
where the time goes in v2:
time: 350 us; the launch traced here: 348 us
  waiting for transfers between devices  181 us (52%)
  Pallas kernels  82.6 us (24%)
  starting transfers between devices  69.6 us (20%)
  other arithmetic  8.55 us (2%)
  local copies, waits for them, and re-layouts  5.23 us (1%)
    ppermute x6, waiting for transfers between devices, to_far(): return lax.ppermute(a, 'tp', FAR)  82.5 us
    ppermute x7, waiting for transfers between devices, to_near(): return lax.ppermute(a, 'tp', NEAR)  52.5 us
    all_to_all x5, starting transfers between devices, swap(): lax.all_to_all(a.reshape(experts, rows // experts, cols), EP, split_axis=...  37.5 us
    pallas_call x1, Pallas kernels, mixer(): pl.pallas_call(mixer_kernel, grid_spec=pltpu.PrefetchScalarGridSpec(num_s...  28.5 us
    all_to_all x5, waiting for transfers between devices, swap(): lax.all_to_all(a.reshape(experts, rows // experts, cols), EP, split_axis=...  19.3 us
    pallas_call x2, Pallas kernels, hidden_units(): pl.pallas_call(hidden_kernel, grid=(width // kb,), in_specs=[pl.BlockSpec...  17.7 us
    ppermute x6, starting transfers between devices, to_far(): return lax.ppermute(a, 'tp', FAR)  14.4 us
    ppermute x3, waiting for transfers between devices, arriving_state(): lax.ppermute(plane, 'ep_0', [(i, i + d) for i in range(count - d)])  14.3 us
  transfers between devices with their start and end apart: 26, of which 17 were waited for; matrix products, arithmetic and copies ran while one was open for 2% of the time, Pallas kernels for 18%

profile of v2, /device:TPU:8, one launch (start us, length us, event | category | flops | bytes accessed | tf_op | source)
XLA Modules:
  0.0 347.7 jit_solution(3503836230932376236)
XLA Ops:
  1.3 6.7 %front.1 = (bf16[128,4096]{1,0:T(8,128)(2,1)}, bf16[32,128]{1,0:T(8,128)(2,1)}, bf16[256,8192]{1,0:T(8,128)(2,1)}) custom-call(s32[4]{0:T(128)} %pad_add_fusion.src, bf16[128,4096]{1,0:T(8,128)(2,1)} %x_ref.1, f32[1,4096]{1,0:T(1,128)} %bitcast.57, bf16[32,4096]{1,0:T(8,128)(2,1)} %bitcast.48, s32[4,2,128]{2,1,0:T(2,128)} %bitcast.50), custom_call_target="tpu_custom_call" | custom-call | tf_op jit(solution)/shard_map/front/pallas_call | solution.py:96
  8.0 8.7 %all-to-all-start = ((bf16[32,8,8192]{2,1,0:T(8,128)(2,1)}), bf16[32,8,8192]{2,1,0:T(8,128)(2,1)}, u32[]{:S(2)}, u32[]{:S(2)}) async-start(bf16[32,8,8192]{2,1,0:T(8,128)(2,1)} %bitcast.45), calls=%async_computation | async-start | bytes 8388608 | tf_op jit(solution)/shard_map/all_to_all | solution.py:456
  16.7 1.6 collective-permute-start.3
  18.6 23.4 %collective-permute-done.3.rows_ref = bf16[128,4096]{1,0:T(8,128)(2,1)S(1)} collective-permute-done((bf16[128,4096]{1,0:T(8,128)(2,1)S(1)}, bf16[128,4096]{1,0:T(8,128)(2,1)S(1)}, u32[]{:S(2)}, u32[]{:S(2)}) %collective-permute-start.3) | collective-permute-done | bytes 1048608 | tf_op jit(solution)/shard_map/ppermute | solution.py:440
  42.0 1.0 copy-done.4
  42.9 5.9 %refill.1 = (bf16[32,128]{1,0:T(8,128)(2,1)}, bf16[256,4096]{1,0:T(8,128)(2,1)}, bf16[256,4096]{1,0:T(8,128)(2,1)}) custom-call(s32[4]{0:T(128)} %pad_add_fusion.src, bf16[128,4096]{1,0:T(8,128)(2,1)} %copy-done.4, bf16[32,4096]{1,0:T(8,128)(2,1)} %bitcast.49, s32[4,2,128]{2,1,0:T(2,128)} %bitcast.51), custom_call_target="tpu_custom_call" | custom-call | tf_op jit(solution)/shard_map/refill/pallas_call | solution.py:128
  48.8 19.3 %all-to-all-done = bf16[32,8,8192]{2,1,0:T(8,128)(2,1)} async-done(((bf16[32,8,8192]{2,1,0:T(8,128)(2,1)}), bf16[32,8,8192]{2,1,0:T(8,128)(2,1)}, u32[]{:S(2)}, u32[]{:S(2)}) %all-to-all-start) | async-done | bytes 4194336 | tf_op jit(solution)/shard_map/all_to_all | solution.py:456
  68.1 6.6 %all-to-all-start.1 = ((bf16[32,8,4096]{2,1,0:T(8,128)(2,1)}), bf16[32,8,4096]{2,1,0:T(8,128)(2,1)S(1)}, u32[]{:S(2)}, u32[]{:S(2)}) async-start(bf16[32,8,4096]{2,1,0:T(8,128)(2,1)} %bitcast.47), calls=%async_computation.1 | async-start | bytes 4194304 | tf_op jit(solution)/shard_map/all_to_all | solution.py:456
  74.8 1.3 fusion.2.a0
  76.1 2.8 collective-permute-start.1
  79.3 2.8 collective-permute-start.13
  82.1 21.4 %collective-permute-done.1.a2 = bf16[128,4096]{1,0:T(8,128)(2,1)S(1)} collective-permute-done((bf16[128,4096]{1,0:T(8,128)(2,1)}, bf16[128,4096]{1,0:T(8,128)(2,1)S(1)}, u32[]{:S(2)}, u32[]{:S(2)}) %collective-permute-start.1) | collective-permute-done | bytes 1048608 | tf_op jit(solution)/shard_map/ppermute | solution.py:444
  105.2 7.5 %all-to-all-start.2 = ((bf16[32,8,4096]{2,1,0:T(8,128)(2,1)}), bf16[32,8,4096]{2,1,0:T(8,128)(2,1)}, u32[]{:S(2)}, u32[]{:S(2)}) async-start(bf16[32,8,4096]{2,1,0:T(8,128)(2,1)} %bitcast.46), calls=%async_computation.2 | async-start | bytes 4194304 | tf_op jit(solution)/shard_map/all_to_all | solution.py:456
  112.7 16.5 %collective-permute-done.2.a3 = bf16[128,4096]{1,0:T(8,128)(2,1)} collective-permute-done((bf16[128,4096]{1,0:T(8,128)(2,1)S(1)}, bf16[128,4096]{1,0:T(8,128)(2,1)}, u32[]{:S(2)}, u32[]{:S(2)}) %collective-permute-start.2) | collective-permute-done | bytes 1048608 | tf_op jit(solution)/shard_map/ppermute | solution.py:440
  129.2 28.5 %mixer.1 = (f32[512,512]{1,0:T(8,128)}, f32[512,512]{1,0:T(8,128)}, f32[4,136,128]{2,1,0:T(8,128)}) custom-call(s32[4]{0:T(128)} %pad_add_fusion.src, bf16[128,4096]{1,0:T(8,128)(2,1)} %fusion.2.a0, bf16[128,4096]{1,0:T(8,128)(2,1)} %collective-permute-done.a1, bf16[128,4096]{1,0:T(8,128)(2,1)} %copy-done.5, bf16[128,4096]{1,0:T(8,128)(2,1)} %collective-permute-done.2.a3, ...), custom_call_target="tpu_custom_call" | custom-call | tf_op jit(solution)/shard_map/mixer/pallas_call | solution.py:207
  157.7 35.0 %collective-permute-done.13.uf_ref = bf16[4096,256]{1,0:T(8,128)(2,1)} collective-permute-done((bf16[4096,256]{1,0:T(8,128)(2,1)}, bf16[4096,256]{1,0:T(8,128)(2,1)}, u32[]{:S(2)}, u32[]{:S(2)}) %collective-permute-start.13) | collective-permute-done | bytes 2097184 | tf_op jit(solution)/shard_map/ppermute | solution.py:444
  192.7 8.8 %hidden.2.h_own = bf16[512,512]{1,0:T(8,128)(2,1)} custom-call(bf16[256,8192]{1,0:T(8,128)(2,1)} %bitcast.11.own_ref, bf16[256,4096]{1,0:T(8,128)(2,1)} %bitcast.44, bf16[4096,256]{1,0:T(8,128)(2,1)} %bitcast.28.go_ref, bf16[4096,256]{1,0:T(8,128)(2,1)} %bitcast.29.uo_ref, bf16[4096,256]{1,0:T(8,128)(2,1)} %collective-permute-done.12.gf_ref, ...), custom_call_target="tpu_custom_call" | custom-call | tf_op jit(solution)/shard_map/hidden/pallas_call | solution.py:337
  201.5 2.8 collective-permute-start.15
  204.3 11.8 %collective-permute-done.15.h_far = bf16[512,512]{1,0:T(8,128)(2,1)S(1)} collective-permute-done((bf16[512,512]{1,0:T(8,128)(2,1)}, bf16[512,512]{1,0:T(8,128)(2,1)S(1)}, u32[]{:S(2)}, u32[]{:S(2)}) %collective-permute-start.15) | collective-permute-done | bytes 524320 | tf_op jit(solution)/shard_map/ppermute | solution.py:444
  216.0 2.0 collective-permute-start.14
  218.1 8.8 %hidden.3.h_own = bf16[512,512]{1,0:T(8,128)(2,1)} custom-call(bf16[256,8192]{1,0:T(8,128)(2,1)} %bitcast.11.own_ref, bf16[256,4096]{1,0:T(8,128)(2,1)} %bitcast.31.near_ref, bf16[4096,256]{1,0:T(8,128)(2,1)} %bitcast.28.go_ref, bf16[4096,256]{1,0:T(8,128)(2,1)} %bitcast.29.uo_ref, bf16[4096,256]{1,0:T(8,128)(2,1)} %collective-permute-done.12.gf_ref, ...), custom_call_target="tpu_custom_call" | custom-call | tf_op jit(solution)/shard_map/hidden/pallas_call | solution.py:337
  226.9 3.9 %collective-permute-done.16.h_opp = bf16[512,512]{1,0:T(8,128)(2,1)S(1)} collective-permute-done((bf16[512,512]{1,0:T(8,128)(2,1)S(1)}, bf16[512,512]{1,0:T(8,128)(2,1)S(1)}, u32[]{:S(2)}, u32[]{:S(2)}) %collective-permute-start.16) | collective-permute-done | bytes 524320 | tf_op jit(solution)/shard_map/ppermute | solution.py:440
  230.8 8.7 %collective-permute-done.14.h_near = bf16[512,512]{1,0:T(8,128)(2,1)S(1)} collective-permute-done((bf16[512,512]{1,0:T(8,128)(2,1)}, bf16[512,512]{1,0:T(8,128)(2,1)S(1)}, u32[]{:S(2)}, u32[]{:S(2)}) %collective-permute-start.14) | collective-permute-done | bytes 524320 | tf_op jit(solution)/shard_map/ppermute | solution.py:440
  240.3 6.8 %down.2 = bf16[256,4096]{1,0:T(8,128)(2,1)} custom-call(s32[4]{0:T(128)} %pad_add_fusion.src, bf16[512,512]{1,0:T(8,128)(2,1)} %hidden.2.h_own, bf16[512,512]{1,0:T(8,128)(2,1)} %copy-done.10, bf16[512,512]{1,0:T(8,128)(2,1)} %copy-done.8, bf16[512,512]{1,0:T(8,128)(2,1)} %copy-done.9, bf16[1024,1024]{1,0:T(8,128)(2,1)} %bitcast.39), custom_call_target="tpu_custom_call" | custom-call | tf_op jit(solution)/shard_map/down/pallas_call | solution.py:377
  247.1 7.6 %all-to-all-start.3 = ((bf16[32,8,4096]{2,1,0:T(8,128)(2,1)}), bf16[32,8,4096]{2,1,0:T(8,128)(2,1)S(1)}, u32[]{:S(2)}, u32[]{:S(2)}) async-start(bf16[32,8,4096]{2,1,0:T(8,128)(2,1)} %bitcast.41), calls=%async_computation.3 | async-start | bytes 4194304 | tf_op jit(solution)/shard_map/all_to_all | solution.py:456
  254.9 2.8 collective-permute-start.18
  258.3 12.1 %collective-permute-done.18.h_far = bf16[512,512]{1,0:T(8,128)(2,1)} collective-permute-done((bf16[512,512]{1,0:T(8,128)(2,1)S(1)}, bf16[512,512]{1,0:T(8,128)(2,1)}, u32[]{:S(2)}, u32[]{:S(2)}) %collective-permute-start.18) | collective-permute-done | bytes 524320 | tf_op jit(solution)/shard_map/ppermute | solution.py:444
  271.2 1.5 collective-permute-start.7
  273.5 2.4 collective-permute-start.5
  275.9 6.1 %collective-permute-done.7 = f32[2,136,128]{2,1,0:T(8,128)} collective-permute-done((f32[2,136,128]{2,1,0:T(8,128)}, f32[2,136,128]{2,1,0:T(8,128)}, u32[]{:S(2)}, u32[]{:S(2)}) %collective-permute-start.7) | collective-permute-done | bytes 139296 | tf_op jit(solution)/shard_map/ppermute | solution.py:288
  282.0 2.3 collective-permute-done.6
  284.3 2.5 collective-permute-done.5
  286.8 1.3 fusion.12
  288.9 6.8 %down.3 = bf16[256,4096]{1,0:T(8,128)(2,1)} custom-call(s32[4]{0:T(128)} %pad_add_fusion.src, bf16[512,512]{1,0:T(8,128)(2,1)} %hidden.3.h_own, bf16[512,512]{1,0:T(8,128)(2,1)} %copy-done.7, bf16[512,512]{1,0:T(8,128)(2,1)} %collective-permute-done.18.h_far, bf16[512,512]{1,0:T(8,128)(2,1)} %collective-permute-done.19.h_opp, bf16[1024,1024]{1,0:T(8,128)(2,1)} %bitcast.40), custom_call_target="tpu_custom_call" | custom-call | tf_op jit(solution)/shard_map/down/pallas_call | solution.py:377
  295.9 1.2 copy-done
  297.1 7.0 %all-to-all-start.4 = ((bf16[32,8,4096]{2,1,0:T(8,128)(2,1)}), bf16[32,8,4096]{2,1,0:T(8,128)(2,1)}, u32[]{:S(2)}, u32[]{:S(2)}) async-start(bf16[32,8,4096]{2,1,0:T(8,128)(2,1)} %bitcast.42), calls=%async_computation.4 | async-start | bytes 4194304 | tf_op jit(solution)/shard_map/all_to_all | solution.py:456
  304.2 1.1 add_add_fusion
  305.3 4.9 %collective-permute-start.9 = (f32[2,136,128]{2,1,0:T(8,128)S(1)}, f32[2,136,128]{2,1,0:T(8,128)S(1)}, u32[]{:S(2)}, u32[]{:S(2)}) collective-permute-start(f32[2,136,128]{2,1,0:T(8,128)S(1)} %pad_maximum_fusion.2), channel_id=1, source_target_pairs={{0,64},{32,96},{1,65},{33,97},{2,66},{34,98},{3,67},{35,99},{4,68}... | collective-permute-start | bytes 417800 | tf_op jit(solution)/shard_map/ppermute | solution.py:297
  310.3 2.8 collective-permute-start.20
  313.1 2.2 collective-permute-done.20
  315.9 2.5 collective-permute-start.8
  318.4 1.3 collective-permute-start.10
  319.7 11.1 %collective-permute-done.9 = f32[2,136,128]{2,1,0:T(8,128)S(1)} collective-permute-done((f32[2,136,128]{2,1,0:T(8,128)S(1)}, f32[2,136,128]{2,1,0:T(8,128)S(1)}, u32[]{:S(2)}, u32[]{:S(2)}) %collective-permute-start.9) | collective-permute-done | bytes 139296 | tf_op jit(solution)/shard_map/ppermute | solution.py:297
  330.9 2.4 collective-permute-done.8
  334.0 1.1 fusion.5
  335.3 1.2 collective-permute-done.11
  337.3 4.4 %readout.1 = bf16[512,512]{1,0:T(8,128)(2,1)} custom-call(f32[512,512]{1,0:T(8,128)} %get-tuple-element.24.inside_ref, f32[512,512]{1,0:T(8,128)} %get-tuple-element.25.query_ref, f32[4,128,128]{2,1,0:T(8,128)} %fusion.3.state_ref, f32[1,512]{1,0:T(1,128)} %bitcast.73), custom_call_target="tpu_custom_call" | custom-call | tf_op jit(solution)/shard_map/readout/pallas_call | solution.py:239
  341.7 6.0 %combine.1 = bf16[512,1024]{1,0:T(8,128)(2,1)} custom-call(s32[4]{0:T(128)} %pad_add_fusion.src, bf16[256,4096]{1,0:T(8,128)(2,1)} %bitcast.43, bf16[256,4096]{1,0:T(8,128)(2,1)} %bitcast.36.high_ref, s32[4,2,128]{2,1,0:T(2,128)} %bitcast.52, bf16[4,32,128]{2,1,0:T(8,128)(2,1)} %pad_maximum_fusion.3.logits_ref), custom_call_target="tpu_custom_call" | custom-call | tf_op jit(solution)/shard_map/combine/pallas_call | solution.py:416
  (88 shorter events, 9.5 us)
Async XLA Ops:
  8.0 8.7 %copy-start.25 = (bf16[128,4096]{1,0:T(8,128)(2,1)S(1)}, bf16[128,4096]{1,0:T(8,128)(2,1)}, u32[]{:S(2)}) copy-start(bf16[128,4096]{1,0:T(8,128)(2,1)} %get-tuple-element.22) | copy-start | bytes 3145732
  8.0 10.3 %copy-start.2 = (bf16[128,4096]{1,0:T(8,128)(2,1)S(1)}, bf16[128,4096]{1,0:T(8,128)(2,1)}, u32[]{:S(2)}) copy-start(bf16[128,4096]{1,0:T(8,128)(2,1)} %param.14) | copy-start | bytes 3145732
  8.0 60.2 %all-to-all-start = ((bf16[32,8,8192]{2,1,0:T(8,128)(2,1)}), bf16[32,8,8192]{2,1,0:T(8,128)(2,1)}, u32[]{:S(2)}, u32[]{:S(2)}) async-start(bf16[32,8,8192]{2,1,0:T(8,128)(2,1)} %bitcast.45), calls=%async_computation | async-start | bytes 8388608 | tf_op jit(solution)/shard_map/all_to_all | solution.py:456
  16.7 25.3 %collective-permute-start.3 = (bf16[128,4096]{1,0:T(8,128)(2,1)S(1)}, bf16[128,4096]{1,0:T(8,128)(2,1)S(1)}, u32[]{:S(2)}, u32[]{:S(2)}) collective-permute-start(bf16[128,4096]{1,0:T(8,128)(2,1)S(1)} %copy-done.25), channel_id=1, source_target_pairs={{0,1},{1,0},{2,3},{3,2},{4,5},{5,4},{6,7},{7,6},{8,9},{9,8},{10,11... | collective-permute-start | bytes 3145736 | tf_op jit(solution)/shard_map/ppermute | solution.py:440
  68.1 6.7 %copy-start.13 = (f32[4096]{0:T(1024)S(1)}, f32[4096]{0:T(1024)}, u32[]{:S(2)}) copy-start(f32[4096]{0:T(1024)} %param.16) | copy-start | bytes 49156
  68.1 35.7 %all-to-all-start.1 = ((bf16[32,8,4096]{2,1,0:T(8,128)(2,1)}), bf16[32,8,4096]{2,1,0:T(8,128)(2,1)S(1)}, u32[]{:S(2)}, u32[]{:S(2)}) async-start(bf16[32,8,4096]{2,1,0:T(8,128)(2,1)} %bitcast.47), calls=%async_computation.1 | async-start | bytes 4194304 | tf_op jit(solution)/shard_map/all_to_all | solution.py:456
  76.1 27.5 %collective-permute-start.1 = (bf16[128,4096]{1,0:T(8,128)(2,1)}, bf16[128,4096]{1,0:T(8,128)(2,1)S(1)}, u32[]{:S(2)}, u32[]{:S(2)}) collective-permute-start(bf16[128,4096]{1,0:T(8,128)(2,1)} %fusion.2.a0), channel_id=1, source_target_pairs={{0,3},{1,2},{2,1},{3,0},{4,7},{5,6},{6,5},{7,4},{8,11},{9,10},{10,... | collective-permute-start | bytes 3145736 | tf_op jit(solution)/shard_map/ppermute | solution.py:444
  78.9 78.9 %collective-permute-start.12 = (bf16[4096,256]{1,0:T(8,128)(2,1)}, bf16[4096,256]{1,0:T(8,128)(2,1)}, u32[]{:S(2)}, u32[]{:S(2)}) collective-permute-start(bf16[4096,256]{1,0:T(8,128)(2,1)} %bitcast.28.go_ref), channel_id=1, source_target_pairs={{0,3},{1,2},{2,1},{3,0},{4,7},{5,6},{6,5},{7,4},{8,11},{9,10},{10,... | collective-permute-start | bytes 6291464 | tf_op jit(solution)/shard_map/ppermute | solution.py:444
  79.3 113.4 %collective-permute-start.13 = (bf16[4096,256]{1,0:T(8,128)(2,1)}, bf16[4096,256]{1,0:T(8,128)(2,1)}, u32[]{:S(2)}, u32[]{:S(2)}) collective-permute-start(bf16[4096,256]{1,0:T(8,128)(2,1)} %bitcast.29.uo_ref), channel_id=1, source_target_pairs={{0,3},{1,2},{2,1},{3,0},{4,7},{5,6},{6,5},{7,4},{8,11},{9,10},{10,... | collective-permute-start | bytes 6291464 | tf_op jit(solution)/shard_map/ppermute | solution.py:444
  82.1 30.6 %collective-permute-start = (bf16[128,4096]{1,0:T(8,128)(2,1)}, bf16[128,4096]{1,0:T(8,128)(2,1)}, u32[]{:S(2)}, u32[]{:S(2)}) collective-permute-start(bf16[128,4096]{1,0:T(8,128)(2,1)} %fusion.2.a0), channel_id=1, source_target_pairs={{0,1},{1,0},{2,3},{3,2},{4,5},{5,4},{6,7},{7,6},{8,9},{9,8},{10,11... | collective-permute-start | bytes 3145736 | tf_op jit(solution)/shard_map/ppermute | solution.py:440
  103.5 25.7 %collective-permute-start.2 = (bf16[128,4096]{1,0:T(8,128)(2,1)S(1)}, bf16[128,4096]{1,0:T(8,128)(2,1)}, u32[]{:S(2)}, u32[]{:S(2)}) collective-permute-start(bf16[128,4096]{1,0:T(8,128)(2,1)S(1)} %collective-permute-done.1.a2), channel_id=1, source_target_pairs={{0,1},{1,0},{2,3},{3,2},{4,5},{5,4},{6,7},{7,6},{8,9},{9,8},{10,11... | collective-permute-start | bytes 3145736 | tf_op jit(solution)/shard_map/ppermute | solution.py:440
  103.8 1.3 copy-start.1
  105.2 112.9 %all-to-all-start.2 = ((bf16[32,8,4096]{2,1,0:T(8,128)(2,1)}), bf16[32,8,4096]{2,1,0:T(8,128)(2,1)}, u32[]{:S(2)}, u32[]{:S(2)}) async-start(bf16[32,8,4096]{2,1,0:T(8,128)(2,1)} %bitcast.46), calls=%async_computation.2 | async-start | bytes 4194304 | tf_op jit(solution)/shard_map/all_to_all | solution.py:456
  201.5 14.5 %collective-permute-start.15 = (bf16[512,512]{1,0:T(8,128)(2,1)}, bf16[512,512]{1,0:T(8,128)(2,1)S(1)}, u32[]{:S(2)}, u32[]{:S(2)}) collective-permute-start(bf16[512,512]{1,0:T(8,128)(2,1)} %hidden.2.h_own), channel_id=1, source_target_pairs={{0,3},{1,2},{2,1},{3,0},{4,7},{5,6},{6,5},{7,4},{8,11},{9,10},{10,... | collective-permute-start | bytes 1572872 | tf_op jit(solution)/shard_map/ppermute | solution.py:444
  216.0 10.9 %copy-start.8 = (bf16[512,512]{1,0:T(8,128)(2,1)}, bf16[512,512]{1,0:T(8,128)(2,1)S(1)}, u32[]{:S(2)}) copy-start(bf16[512,512]{1,0:T(8,128)(2,1)S(1)} %collective-permute-done.15.h_far) | copy-start | bytes 1572868
  216.0 14.8 %collective-permute-start.16 = (bf16[512,512]{1,0:T(8,128)(2,1)S(1)}, bf16[512,512]{1,0:T(8,128)(2,1)S(1)}, u32[]{:S(2)}, u32[]{:S(2)}) collective-permute-start(bf16[512,512]{1,0:T(8,128)(2,1)S(1)} %collective-permute-done.15.h_far), channel_id=1, source_target_pairs={{0,1},{1,0},{2,3},{3,2},{4,5},{5,4},{6,7},{7,6},{8,9},{9,8},{10,11... | collective-permute-start | bytes 1572872 | tf_op jit(solution)/shard_map/ppermute | solution.py:440
  216.0 23.5 %collective-permute-start.14 = (bf16[512,512]{1,0:T(8,128)(2,1)}, bf16[512,512]{1,0:T(8,128)(2,1)S(1)}, u32[]{:S(2)}, u32[]{:S(2)}) collective-permute-start(bf16[512,512]{1,0:T(8,128)(2,1)} %hidden.2.h_own), channel_id=1, source_target_pairs={{0,1},{1,0},{2,3},{3,2},{4,5},{5,4},{6,7},{7,6},{8,9},{9,8},{10,11... | collective-permute-start | bytes 1572872 | tf_op jit(solution)/shard_map/ppermute | solution.py:440
  230.8 8.7 %copy-start.9 = (bf16[512,512]{1,0:T(8,128)(2,1)}, bf16[512,512]{1,0:T(8,128)(2,1)S(1)}, u32[]{:S(2)}) copy-start(bf16[512,512]{1,0:T(8,128)(2,1)S(1)} %collective-permute-done.16.h_opp) | copy-start | bytes 1572868
  247.1 7.6 %copy-start.6 = (f32[4,136,128]{2,1,0:T(8,128)S(1)}, f32[4,136,128]{2,1,0:T(8,128)}, u32[]{:S(2)}) copy-start(f32[4,136,128]{2,1,0:T(8,128)} %get-tuple-element.32) | copy-start | bytes 835588
  247.1 7.8 %copy-start.3 = (bf16[512,512]{1,0:T(8,128)(2,1)S(1)}, bf16[512,512]{1,0:T(8,128)(2,1)}, u32[]{:S(2)}) copy-start(bf16[512,512]{1,0:T(8,128)(2,1)} %hidden.3.h_own) | copy-start | bytes 1572868
  247.1 48.7 %all-to-all-start.3 = ((bf16[32,8,4096]{2,1,0:T(8,128)(2,1)}), bf16[32,8,4096]{2,1,0:T(8,128)(2,1)S(1)}, u32[]{:S(2)}, u32[]{:S(2)}) async-start(bf16[32,8,4096]{2,1,0:T(8,128)(2,1)} %bitcast.41), calls=%async_computation.3 | async-start | bytes 4194304 | tf_op jit(solution)/shard_map/all_to_all | solution.py:456
  254.7 3.0 collective-permute-start.4
  254.9 15.5 %collective-permute-start.18 = (bf16[512,512]{1,0:T(8,128)(2,1)S(1)}, bf16[512,512]{1,0:T(8,128)(2,1)}, u32[]{:S(2)}, u32[]{:S(2)}) collective-permute-start(bf16[512,512]{1,0:T(8,128)(2,1)S(1)} %copy-done.3), channel_id=1, source_target_pairs={{0,3},{1,2},{2,1},{3,0},{4,7},{5,6},{6,5},{7,4},{8,11},{9,10},{10,... | collective-permute-start | bytes 1572872 | tf_op jit(solution)/shard_map/ppermute | solution.py:444
  258.3 12.8 %copy-start.16 = (f32[2,1,128]{2,1,0:T(1,128)}, f32[2,1,128]{2,1,0:T(1,128)S(1)}, u32[]{:S(2)}) copy-start(f32[2,1,128]{2,1,0:T(1,128)S(1)} %get-tuple-element.47) | copy-start | bytes 3076
  258.3 29.8 %collective-permute-start.17 = (bf16[512,512]{1,0:T(8,128)(2,1)S(1)}, bf16[512,512]{1,0:T(8,128)(2,1)S(1)}, u32[]{:S(2)}, u32[]{:S(2)}) collective-permute-start(bf16[512,512]{1,0:T(8,128)(2,1)S(1)} %copy-done.3), channel_id=1, source_target_pairs={{0,1},{1,0},{2,3},{3,2},{4,5},{5,4},{6,7},{7,6},{8,9},{9,8},{10,11... | collective-permute-start | bytes 1572872 | tf_op jit(solution)/shard_map/ppermute | solution.py:440
  270.5 17.7 %collective-permute-start.19 = (bf16[512,512]{1,0:T(8,128)(2,1)}, bf16[512,512]{1,0:T(8,128)(2,1)}, u32[]{:S(2)}, u32[]{:S(2)}) collective-permute-start(bf16[512,512]{1,0:T(8,128)(2,1)} %collective-permute-done.18.h_far), channel_id=1, source_target_pairs={{0,1},{1,0},{2,3},{3,2},{4,5},{5,4},{6,7},{7,6},{8,9},{9,8},{10,11... | collective-permute-start | bytes 1572872 | tf_op jit(solution)/shard_map/ppermute | solution.py:440
  271.2 10.8 %collective-permute-start.7 = (f32[2,136,128]{2,1,0:T(8,128)}, f32[2,136,128]{2,1,0:T(8,128)}, u32[]{:S(2)}, u32[]{:S(2)}) collective-permute-start(f32[2,136,128]{2,1,0:T(8,128)} %pad_maximum_fusion.1), channel_id=1, source_target_pairs={{0,8},{8,16},{16,24},{24,0},{1,9},{9,17},{17,25},{25,1},{2,10},{10... | collective-permute-start | bytes 417800 | tf_op jit(solution)/shard_map/ppermute | solution.py:288
  272.6 11.7 %collective-permute-start.6 = (f32[2,136,128]{2,1,0:T(8,128)}, f32[2,136,128]{2,1,0:T(8,128)}, u32[]{:S(2)}, u32[]{:S(2)}) collective-permute-start(f32[2,136,128]{2,1,0:T(8,128)} %pad_maximum_fusion.1), channel_id=1, source_target_pairs={{0,16},{8,24},{16,0},{24,8},{1,17},{9,25},{17,1},{25,9},{2,18},{10... | collective-permute-start | bytes 417800 | tf_op jit(solution)/shard_map/ppermute | solution.py:288
  273.5 13.3 %collective-permute-start.5 = (f32[2,136,128]{2,1,0:T(8,128)}, f32[2,136,128]{2,1,0:T(8,128)}, u32[]{:S(2)}, u32[]{:S(2)}) collective-permute-start(f32[2,136,128]{2,1,0:T(8,128)} %pad_maximum_fusion.1), channel_id=1, source_target_pairs={{0,24},{8,0},{16,8},{24,16},{1,25},{9,1},{17,9},{25,17},{2,26},{10... | collective-permute-start | bytes 417800 | tf_op jit(solution)/shard_map/ppermute | solution.py:288
  295.7 1.4 copy-start
  295.7 8.3 %copy-start.17 = (f32[2,1,128]{2,1,0:T(1,128)S(1)}, f32[2,1,128]{2,1,0:T(1,128)}, u32[]{:S(2)}) copy-start(f32[2,1,128]{2,1,0:T(1,128)} %copy-done.16) | copy-start | bytes 3076
  295.7 8.3 %copy-start.23 = (f32[2,1,128]{2,1,0:T(1,128)S(1)}, f32[2,1,128]{2,1,0:T(1,128)}, u32[]{:S(2)}) copy-start(f32[2,1,128]{2,1,0:T(1,128)} %get-tuple-element.55) | copy-start | bytes 3076
  295.8 8.3 %copy-start.24 = (f32[2,1,128]{2,1,0:T(1,128)S(1)}, f32[2,1,128]{2,1,0:T(1,128)}, u32[]{:S(2)}) copy-start(f32[2,1,128]{2,1,0:T(1,128)} %get-tuple-element.57) | copy-start | bytes 3076
  295.8 8.3 %copy-start.14 = (f32[2,1,128]{2,1,0:T(1,128)S(1)}, f32[2,1,128]{2,1,0:T(1,128)}, u32[]{:S(2)}) copy-start(f32[2,1,128]{2,1,0:T(1,128)} %get-tuple-element.52) | copy-start | bytes 3076
  295.8 8.3 %copy-start.15 = (f32[2,1,128]{2,1,0:T(1,128)S(1)}, f32[2,1,128]{2,1,0:T(1,128)}, u32[]{:S(2)}) copy-start(f32[2,1,128]{2,1,0:T(1,128)} %get-tuple-element.58) | copy-start | bytes 3076
  295.8 8.3 %copy-start.19 = (f32[2,1,128]{2,1,0:T(1,128)S(1)}, f32[2,1,128]{2,1,0:T(1,128)}, u32[]{:S(2)}) copy-start(f32[2,1,128]{2,1,0:T(1,128)} %get-tuple-element.53) | copy-start | bytes 3076
  295.8 8.3 %copy-start.20 = (f32[2,1,128]{2,1,0:T(1,128)S(1)}, f32[2,1,128]{2,1,0:T(1,128)}, u32[]{:S(2)}) copy-start(f32[2,1,128]{2,1,0:T(1,128)} %get-tuple-element.54) | copy-start | bytes 3076
  295.8 8.3 %copy-start.21 = (f32[2,1,128]{2,1,0:T(1,128)S(1)}, f32[2,1,128]{2,1,0:T(1,128)}, u32[]{:S(2)}) copy-start(f32[2,1,128]{2,1,0:T(1,128)} %get-tuple-element.59) | copy-start | bytes 3076
  295.8 8.3 %copy-start.22 = (f32[2,1,128]{2,1,0:T(1,128)S(1)}, f32[2,1,128]{2,1,0:T(1,128)}, u32[]{:S(2)}) copy-start(f32[2,1,128]{2,1,0:T(1,128)} %get-tuple-element.46) | copy-start | bytes 3076
  295.8 14.4 %copy-start.11 = (bf16[32,128]{1,0:T(8,128)(2,1)S(1)}, bf16[32,128]{1,0:T(8,128)(2,1)}, u32[]{:S(2)}) copy-start(bf16[32,128]{1,0:T(8,128)(2,1)} %get-tuple-element.40) | copy-start | bytes 24580
  295.8 14.4 %copy-start.12 = (bf16[32,128]{1,0:T(8,128)(2,1)S(1)}, bf16[32,128]{1,0:T(8,128)(2,1)}, u32[]{:S(2)}) copy-start(bf16[32,128]{1,0:T(8,128)(2,1)} %get-tuple-element.41) | copy-start | bytes 24580
  295.9 38.2 %copy-start.18 = (f32[2,1,128]{2,1,0:T(1,128)S(1)}, f32[2,1,128]{2,1,0:T(1,128)}, u32[]{:S(2)}) copy-start(f32[2,1,128]{2,1,0:T(1,128)} %get-tuple-element.56) | copy-start | bytes 3076
  297.1 44.6 %all-to-all-start.4 = ((bf16[32,8,4096]{2,1,0:T(8,128)(2,1)}), bf16[32,8,4096]{2,1,0:T(8,128)(2,1)}, u32[]{:S(2)}, u32[]{:S(2)}) async-start(bf16[32,8,4096]{2,1,0:T(8,128)(2,1)} %bitcast.42), calls=%async_computation.4 | async-start | bytes 4194304 | tf_op jit(solution)/shard_map/all_to_all | solution.py:456
  305.3 25.5 %collective-permute-start.9 = (f32[2,136,128]{2,1,0:T(8,128)S(1)}, f32[2,136,128]{2,1,0:T(8,128)S(1)}, u32[]{:S(2)}, u32[]{:S(2)}) collective-permute-start(f32[2,136,128]{2,1,0:T(8,128)S(1)} %pad_maximum_fusion.2), channel_id=1, source_target_pairs={{0,64},{32,96},{1,65},{33,97},{2,66},{34,98},{3,67},{35,99},{4,68}... | collective-permute-start | bytes 417800 | tf_op jit(solution)/shard_map/ppermute | solution.py:297
  310.3 5.0 %collective-permute-start.20 = (bf16[2,32,128]{2,1,0:T(8,128)(2,1)S(1)}, bf16[2,32,128]{2,1,0:T(8,128)(2,1)S(1)}, u32[]{:S(2)}, u32[]{:S(2)}) collective-permute-start(bf16[2,32,128]{2,1,0:T(8,128)(2,1)S(1)} %pad_maximum_fusion.4), channel_id=1, source_target_pairs={{0,3},{1,2},{2,1},{3,0},{4,7},{5,6},{6,5},{7,4},{8,11},{9,10},{10,... | collective-permute-start | bytes 49160 | tf_op jit(solution)/shard_map/ppermute | solution.py:444
  315.9 17.4 %collective-permute-start.8 = (f32[2,136,128]{2,1,0:T(8,128)S(1)}, f32[2,136,128]{2,1,0:T(8,128)S(1)}, u32[]{:S(2)}, u32[]{:S(2)}) collective-permute-start(f32[2,136,128]{2,1,0:T(8,128)S(1)} %pad_maximum_fusion.2), channel_id=1, source_target_pairs={{0,32},{32,64},{64,96},{1,33},{33,65},{65,97},{2,34},{34,66},{66,9... | collective-permute-start | bytes 417800 | tf_op jit(solution)/shard_map/ppermute | solution.py:297
  318.4 15.6 %collective-permute-start.10 = (f32[2,136,128]{2,1,0:T(8,128)S(1)}, f32[2,136,128]{2,1,0:T(8,128)S(1)}, u32[]{:S(2)}, u32[]{:S(2)}) collective-permute-start(f32[2,136,128]{2,1,0:T(8,128)S(1)} %pad_maximum_fusion.2), channel_id=1, source_target_pairs={{0,96},{1,97},{2,98},{3,99},{4,100},{5,101},{6,102},{7,103},{8,104... | collective-permute-start | bytes 417800 | tf_op jit(solution)/shard_map/ppermute | solution.py:297
  335.1 1.4 collective-permute-start.11
  (4 other events, 3.5 us)
